TPU v7x, 512 devices: a whole 4x8x8 slice. The times are simulated.
512 devices in a mesh: sp: 64 (over z, y), tp: 8 (over x, core).
Axes of the slice: x: 4, y: 8, z: 8, core: 2. Of those that a mesh axis runs over, the one named last changes fastest.
Arguments:
- hidden_in: bfloat16 [24576, 2048], P('sp'), may hold values from -6 to 6
- drive: bfloat16 [24576, 1024], P('sp', 'tp'), may hold values from -24 to 24
- wide_poles: float32 [2, 32, 64], P(None, 'tp'), may hold values from -2 to 256, as said below
- narrow_poles: float32 [2, 32, 32], P(None, 'tp'), may hold values from -2 to 128, as said below
- log_step: float32 [32, 2], P('tp'), may hold values from -3.912 to -2.526
- forget: float32 [32, 2, 24576], P('tp', None, 'sp'), may hold values from 0 to 2
- wide_input: bfloat16 [2, 32, 64, 16], P(None, 'tp'), may hold values from -1 to 1
- narrow_input: bfloat16 [2, 32, 32, 16], P(None, 'tp'), may hold values from -1 to 1
- wide_output: bfloat16 [2, 32, 16, 64], P(None, 'tp'), may hold values from -0.5 to 0.5
- narrow_output: bfloat16 [2, 32, 16, 32], P(None, 'tp'), may hold values from -0.75 to 0.75
- skip: float32 [1024], P('tp'), may hold values from -4 to 4
- mix_gain: float32 [1024], P('tp'), may hold values from 0.1 to 1.9
- out_weight: bfloat16 [1024, 2048], P('tp'), may hold values from -0.1875 to 0.1875
- mlp_gain: float32 [2048], replicated, may hold values from 0.1 to 1.9
- up_weight: bfloat16 [2048, 8192], P('sp', 'tp'), may hold values from -0.125 to 0.125
- down_weight: bfloat16 [2048, 8192], P('sp', 'tp'), may hold values from -0.0625 to 0.0625
Outputs:
- hidden_out: bfloat16 [24576, 2048], P('sp')
Inputs may be any that keep to these rules, and one draw needn't show every extreme that they name: `wide_poles`: entry 0 holds real parts, each at most -1 / 24576; entry 1 holds imaginary parts. `narrow_poles`: entry 0 holds real parts, each at most -1 / 24576; entry 1 holds imaginary parts.
All inputs are finite; a program needn't handle non-finite values.
Results may differ from a plain program's by a relative error of at most 0.02.
Values may be sent and summed in bfloat16 or wider, within the bound.
A program may use at most 64 MiB of HBM per device.

v0:
```python
import jax
import jax.numpy as jnp
from jax import lax
from jax.sharding import PartitionSpec as P

epsilon = 1e-06


def copy_for_each(value, axis):
    count = lax.axis_size(axis)
    return lax.all_to_all(
        jnp.broadcast_to(value[None], (count, *value.shape)), axis, 0, 0, tiled=True
    )


def gathered_once(value, axis):
    leaves = jax.tree.leaves(value)
    turns = sorted(range(len(leaves)), key=lambda k: -leaves[k].size)
    width = (1, *leaves[turns[0]].shape)[-1]
    lines = [
        jnp.pad(leaves[k].reshape(-1), (0, -leaves[k].size % width)).reshape(-1, width)
        for k in turns
    ]
    both, at, found = (copy_for_each(jnp.concatenate(lines), axis), 0, {})
    for k, line in zip(turns, lines):
        slab = both[:, at : at + len(line)].reshape(len(both), -1)
        found[k] = slab[:, : leaves[k].size].reshape(-1, *leaves[k].shape)
        at += len(line)
    numbers = iter(range(len(leaves)))
    return jax.tree.map(lambda _: found[next(numbers)], value)


def joined_by_halves(pieces, combine):
    while len(jax.tree.leaves(pieces)[0]) > 1:
        pieces = jax.vmap(combine)(
            *(jax.tree.map(lambda part: part[side::2], pieces) for side in (0, 1))
        )
    return jax.tree.map(lambda part: part[0], pieces)


def carried_in(value, axis, combine, identity):
    count, here = (lax.axis_size(axis), lax.axis_index(axis))
    passed = jnp.arange(count) < here

    def kept(part, zero, own):
        part = jnp.where(
            passed.reshape(-1, *(1 for _ in own.shape)), part, jnp.asarray(zero, own.dtype)
        )
        return part

    pieces = gathered_once(value, axis)
    return joined_by_halves(jax.tree.map(kept, pieces, identity, value), combine)


def of_everyone(value, axis):
    return copy_for_each(value, axis).sum(axis=0)


def split_up(value, dim, count):
    dims = value.shape
    pieces = value.reshape(*dims[:dim], count, dims[dim] // count, *dims[dim + 1 :])
    return jnp.moveaxis(pieces, dim, 0)


def sum_at_owner(value, axis, dim):
    count = lax.axis_size(axis)
    pieces = lax.all_to_all(split_up(value, dim, count), axis, 0, 0, tiled=True)
    return jnp.sum(pieces.astype(jnp.float32), axis=0)


def in_order(pieces, dim):
    pieces = jnp.moveaxis(pieces, 0, dim)
    dims = pieces.shape
    return pieces.reshape(*dims[:dim], dims[dim] * dims[dim + 1], *dims[dim + 2 :])


def collect(value, axis, dim):
    pieces = copy_for_each(value, axis)
    return in_order(pieces, dim)


def combine(earlier, later):
    return (
        later[0] * earlier[0] - later[1] * earlier[1],
        later[0] * earlier[1] + later[1] * earlier[0],
        later[0] * earlier[2] - later[1] * earlier[3] + later[2],
        later[0] * earlier[3] + later[1] * earlier[2] + later[3],
    )


def combine_both(earlier, later):
    return combine(earlier[:4], later[:4]) + combine(earlier[4:], later[4:])


def discretize(pole_pair, log_rate):
    step_size = jnp.exp(log_rate)[:, None]
    growth = pole_pair[0] * step_size
    angle = pole_pair[1] * step_size
    rise_real = jnp.expm1(growth) * jnp.cos(angle) - 2.0 * jnp.sin(0.5 * angle) ** 2
    rise_imag = jnp.exp(growth) * jnp.sin(angle)
    denominator = pole_pair[0] ** 2 + pole_pair[1] ** 2
    coef_real = (rise_real * pole_pair[0] + rise_imag * pole_pair[1]) / denominator
    coef_imag = (rise_imag * pole_pair[0] - rise_real * pole_pair[1]) / denominator
    return (growth.reshape(-1), angle.reshape(-1), coef_real.reshape(-1), coef_imag.reshape(-1))


def kind_states(drive, forget_kind, pole_pair, log_rate, in_weight, kind_index):
    pair_count, state_len = (pole_pair.shape[1], pole_pair.shape[2])
    growth, angle, coef_real, coef_imag = discretize(pole_pair, log_rate)
    diagonal = jnp.eye(pair_count, dtype=jnp.bfloat16)
    select = (jnp.arange(2) == kind_index).astype(jnp.bfloat16)
    in_block = jnp.einsum("pq,k,rpsh->pkhrqs", diagonal, select, in_weight).reshape(
        pair_count * 2 * in_weight.shape[3], 2 * pair_count * state_len
    )
    pushed = jnp.dot(drive, in_block, preferred_element_type=jnp.float32)
    width = pair_count * state_len
    drive_real = pushed[:, :width]
    drive_imag = pushed[:, width:]
    push_real = coef_real * drive_real - coef_imag * drive_imag
    push_imag = coef_real * drive_imag + coef_imag * drive_real
    spread = jnp.repeat(jnp.eye(pair_count, dtype=jnp.float32), state_len, axis=1)
    decay_rows = lax.dot_general(forget_kind, spread, (((0,), (0,)), ((), ())))
    spike_magnitude = jnp.exp(growth[None] - decay_rows)
    return lax.associative_scan(
        combine,
        (
            spike_magnitude * jnp.cos(angle)[None],
            spike_magnitude * jnp.sin(angle)[None],
            push_real,
            push_imag,
        ),
        axis=0,
    )


def read_out(state_real, state_imag, out_kind, kind_index):
    pair_count, group_len, state_len = (out_kind.shape[1], out_kind.shape[2], out_kind.shape[3])
    diagonal = jnp.eye(pair_count, dtype=jnp.float32)
    select = (jnp.arange(2) == kind_index).astype(jnp.float32)
    total_columns = pair_count * 2 * group_len

    def out_block(part_index):
        return jnp.einsum(
            "qp,k,pgs->qspkg", diagonal, select, out_kind[part_index].astype(jnp.float32)
        ).reshape(pair_count * state_len, total_columns)

    first = jnp.dot(state_real, out_block(0))
    second = jnp.dot(state_imag, out_block(1))
    return first - second


def row_norm(rows_in, gain):
    values = rows_in.astype(jnp.float32)
    return (
        values * lax.rsqrt(jnp.mean(values * values, axis=1, keepdims=True) + epsilon) * gain
    ).astype(jnp.bfloat16)


def local(
    hidden_in,
    drive,
    wide_poles,
    narrow_poles,
    log_step,
    forget,
    wide_input,
    narrow_input,
    wide_output,
    narrow_output,
    skip,
    mix_gain,
    out_weight,
    mlp_gain,
    up_weight,
    down_weight,
):
    row_count = drive.shape[0]
    up_whole, down_whole = (
        lax.all_gather(up_weight, "sp", axis=0, tiled=True),
        lax.all_gather(down_weight, "sp", axis=0, tiled=True),
    )
    kinds = ((wide_poles, wide_input, wide_output), (narrow_poles, narrow_input, narrow_output))
    scanned = [
        kind_states(
            drive,
            forget[:, kind_index, :],
            kinds[kind_index][0],
            log_step[:, kind_index],
            kinds[kind_index][1],
            kind_index,
        )
        for kind_index in range(2)
    ]
    ends = tuple((member[-1] for member in scanned[0])) + tuple(
        (member[-1] for member in scanned[1])
    )
    identity = tuple(
        (
            jnp.ones_like(member) if position % 4 == 0 else jnp.zeros_like(member)
            for position, member in enumerate(ends)
        )
    )
    entering = carried_in(ends, "sp", combine_both, identity)
    response = skip[None, :] * drive.astype(jnp.float32)
    for kind_index in range(2):
        cum_real, cum_imag, local_real, local_imag = scanned[kind_index]
        start_real = entering[4 * kind_index + 2][None]
        start_imag = entering[4 * kind_index + 3][None]
        state_real = local_real + cum_real * start_real - cum_imag * start_imag
        state_imag = local_imag + cum_real * start_imag + cum_imag * start_real
        response = response + read_out(state_real, state_imag, kinds[kind_index][2], kind_index)
    active = jax.nn.gelu(response, approximate=False)
    power = of_everyone(jnp.sum(active * active, axis=1), "tp")
    channel_total = drive.shape[1] * lax.axis_size("tp")
    mixed = (active * lax.rsqrt(power / channel_total + epsilon)[:, None] * mix_gain).astype(
        jnp.bfloat16
    )
    share = row_count // lax.axis_size("tp")
    proj_sum = sum_at_owner(
        jnp.dot(mixed, out_weight, preferred_element_type=jnp.float32).astype(jnp.bfloat16), "tp", 0
    )
    own_rows = lax.dynamic_slice_in_dim(hidden_in, lax.axis_index("tp") * share, share, 0)
    carried_rows = (own_rows.astype(jnp.float32) + proj_sum).astype(jnp.bfloat16)
    gathered = collect(row_norm(carried_rows, mlp_gain), "tp", 0)
    pre_act = jnp.dot(gathered, up_whole, preferred_element_type=jnp.float32)
    squared = jnp.square(jax.nn.relu(pre_act)).astype(jnp.bfloat16)
    partial_value = lax.dot_general(
        squared, down_whole, (((1,), (1,)), ((), ())), preferred_element_type=jnp.float32
    )
    mixer_sum = sum_at_owner(partial_value.astype(jnp.bfloat16), "tp", 0)
    completed_result = (carried_rows.astype(jnp.float32) + mixer_sum).astype(jnp.bfloat16)
    return collect(completed_result, "tp", 0)


def solution(mesh):
    return jax.shard_map(
        local,
        mesh=mesh,
        in_specs=(
            P("sp", None),
            P("sp", "tp"),
            P(None, "tp", None),
            P(None, "tp", None),
            P("tp", None),
            P("tp", None, "sp"),
            P(None, "tp", None, None),
            P(None, "tp", None, None),
            P(None, "tp", None, None),
            P(None, "tp", None, None),
            P("tp"),
            P("tp"),
            P("tp", None),
            P(),
            P("sp", "tp"),
            P("sp", "tp"),
        ),
        out_specs=P("sp", None),
        check_vma=False,
    )
```

profile of v0, /device:TPU:1, one launch (start us, length us, event | category | flops | bytes accessed | tf_op | source)
XLA Modules:
  0.0 431.1 jit_solution(17403516793321845758)
XLA Ops:
  55.4 1.5 multiply_subtract_fusion.3
  62.2 1.9 add_add_fusion.5
  68.0 1.5 slice.1383
  69.5 1.5 slice.1392
  71.0 1.7 multiply_subtract_fusion.11
  73.9 1.4 slice.1389
  75.3 1.4 slice.1396
  76.7 1.4 slice.1391
  78.1 1.4 slice.1397
  79.5 1.4 slice.1393
  80.9 1.4 slice.1402
  82.3 1.5 add_add_fusion.14
  93.0 1.5 multiply_subtract_fusion.20
  105.0 1.4 add_add_fusion.26
  139.5 1.4 slice.1388
  140.9 1.4 slice.1455
  142.9 1.4 slice.1463
  147.4 1.5 slice.1469
  195.0 1.6 pad.434
  196.7 1.6 pad.433
  203.7 17.3 %all-to-all-start = ((f32[64,8,256]{2,1,0:T(8,128)}), f32[64,8,256]{2,1,0:T(8,128)S(1)}, u32[]{:S(2)}, u32[]{:S(2)}) async-start(f32[64,8,256]{2,1,0:T(8,128)} %broadcast_in_dim.98), calls=%async_computation | async-start | bytes 1048576 | tf_op jit(solution)/shard_map/all_to_all | solution.py:11
  223.5 1.6 reshape.360
  226.7 1.7 reshape.352
  228.4 1.7 reshape.354
  230.8 7.7 %all-to-all-done = f32[64,8,256]{2,1,0:T(8,128)S(1)} async-done(((f32[64,8,256]{2,1,0:T(8,128)}), f32[64,8,256]{2,1,0:T(8,128)S(1)}, u32[]{:S(2)}, u32[]{:S(2)}) %all-to-all-start) | async-done | bytes 524320 | tf_op jit(solution)/shard_map/all_to_all | solution.py:11
  250.3 1.5 slice.1680
  251.8 1.4 slice.1681
  253.2 1.4 slice.1700
  254.7 1.4 slice.1703
  256.1 1.4 slice.1702
  257.6 1.5 slice.1705
  259.0 1.5 multiply_subtract_fusion.12
  263.3 1.4 slice.1684
  264.6 1.4 slice.1685
  266.0 1.4 slice.1704
  267.4 1.4 slice.1707
  270.1 1.4 slice.1709
  271.4 1.5 multiply_subtract_fusion.18
  282.0 1.4 multiply_subtract_fusion.24
  296.9 1.5 fusion.31
  301.3 11.9 %all_to_all.31 = f32[8,1,384]{2,1,0:T(1,128)S(1)} all-to-all(f32[8,1,384]{2,1,0:T(1,128)S(1)} %broadcast_in_dim.104), channel_id=1, replica_groups=mesh['sp'=64,'tp'=8] {'tp'}, dimensions={0} | all-to-all | bytes 24576 | tf_op jit(solution)/shard_map/all_to_all | solution.py:11
  313.3 1.8 convolution_convert_fusion.1
  315.1 4.2 all-to-all-start.2
  319.3 20.6 %all-to-all-done.2 = bf16[8,48,2048]{2,1,0:T(8,128)(2,1)S(1)} async-done(((bf16[8,48,2048]{2,1,0:T(8,128)(2,1)}), bf16[8,48,2048]{2,1,0:T(8,128)(2,1)S(1)}, u32[]{:S(2)}, u32[]{:S(2)}) %all-to-all-start.2) | async-done | bytes 1572896 | tf_op jit(solution)/shard_map/all_to_all | solution.py:67
  341.6 23.9 %all_to_all.32 = bf16[8,48,2048]{2,1,0:T(8,128)(2,1)S(1)} all-to-all(bf16[8,48,2048]{2,1,0:T(8,128)(2,1)S(1)} %broadcast_in_dim.105), channel_id=1, replica_groups=mesh['sp'=64,'tp'=8] {'tp'}, dimensions={0} | all-to-all | bytes 3145728 | tf_op jit(solution)/shard_map/all_to_all | solution.py:11
  365.5 8.0 %convolution_convert_fusion = bf16[384,2048]{1,0:T(8,128)(2,1)} fusion(bf16[2048,1024]{1,0:T(8,128)(2,1)} %all-gather.5.cloned.1.call-done, bf16[384,2048]{1,0:T(8,128)(2,1)S(1)} %bitcast.131, bf16[2048,1024]{1,0:T(8,128)(2,1)} %all-gather.3.cloned.1.call-done), kind=kOutput, calls=%fused_computation.2 | convolution fusion | flops 3223191552 | bytes 11534336 | tf_op jit(solution)/shard_map/dot_general | solution.py:227
  373.6 25.1 %all_to_all.33 = bf16[8,48,2048]{2,1,0:T(8,128)(2,1)S(1)} all-to-all(bf16[8,48,2048]{2,1,0:T(8,128)(2,1)} %bitcast.132), channel_id=1, replica_groups=mesh['sp'=64,'tp'=8] {'tp'}, dimensions={0} | all-to-all | bytes 3145728 | tf_op jit(solution)/shard_map/all_to_all | solution.py:67
  399.1 24.0 %all_to_all.34 = bf16[8,48,2048]{2,1,0:T(8,128)(2,1)S(1)} all-to-all(bf16[8,48,2048]{2,1,0:T(8,128)(2,1)S(1)} %broadcast_in_dim.106), channel_id=1, replica_groups=mesh['sp'=64,'tp'=8] {'tp'}, dimensions={0} | all-to-all | bytes 3145728 | tf_op jit(solution)/shard_map/all_to_all | solution.py:11
  (932 shorter events, 212.9 us)
Async XLA Ops:
  6.5 306.8 %copy-start = (bf16[128,2048]{1,0:T(8,128)(2,1)S(1)}, bf16[128,2048]{1,0:T(8,128)(2,1)}, u32[]{:S(2)}) copy-start(bf16[128,2048]{1,0:T(8,128)(2,1)} %param.28) | copy-start | bytes 1572868
  6.5 5.5 %copy-start.3 = (bf16[384,128]{1,0:T(8,128)(2,1)S(1)}, bf16[384,128]{1,0:T(8,128)(2,1)}, u32[]{:S(2)}) copy-start(bf16[384,128]{1,0:T(8,128)(2,1)} %param.17) | copy-start | bytes 294916
  6.5 359.0 %all-gather.3.cloned.1.call-start = ((), (), s32[]{:S(2)}) async-start(), calls=%async_computation.6 | async-start | bytes 4259840 | tf_op jit(solution)/shard_map/all_gather | solution.py:179
  12.6 35.8 %copy-start.117 = (f32[2,4,64]{2,1,0:T(4,128)S(1)}, f32[2,4,64]{2,1,0:T(4,128)}, u32[]{:S(2)}) copy-start(f32[2,4,64]{2,1,0:T(4,128)} %param.18) | copy-start | bytes 6148
  39.5 12.2 %copy-start.63 = (bf16[2,4,64,16]{2,3,1,0:T(8,128)(2,1)S(1)}, bf16[2,4,64,16]{2,3,1,0:T(8,128)(2,1)}, u32[]{:S(2)}) copy-start(bf16[2,4,64,16]{2,3,1,0:T(8,128)(2,1)} %param.22) | copy-start | bytes 49156
  64.2 82.0 %copy-start.16 = (f32[96,256]{1,0:T(8,128)}, f32[96,256]{1,0:T(8,128)S(1)}, u32[]{:S(2)}) copy-start(f32[96,256]{1,0:T(8,128)S(1)} %get-tuple-element.86) | copy-start | bytes 294916
  156.2 29.5 %copy-start.135 = (f32[1,128]{1,0:T(1,128)S(1)}, f32[1,128]{1,0:T(1,128)}, u32[]{:S(2)}) copy-start(f32[1,128]{1,0:T(1,128)} %slice.1893) | copy-start | bytes 1540
  156.2 29.6 %copy-start.34 = (f32[47,128]{1,0:T(8,128)S(1)}, f32[47,128]{1,0:T(8,128)}, u32[]{:S(2)}) copy-start(f32[47,128]{1,0:T(8,128)} %slice.1531) | copy-start | bytes 72196
  156.2 29.6 %copy-start.35 = (f32[47,128]{1,0:T(8,128)S(1)}, f32[47,128]{1,0:T(8,128)}, u32[]{:S(2)}) copy-start(f32[47,128]{1,0:T(8,128)} %slice.1582) | copy-start | bytes 72196
  156.2 29.6 %copy-start.51 = (f32[47,128]{1,0:T(8,128)S(1)}, f32[47,128]{1,0:T(8,128)}, u32[]{:S(2)}) copy-start(f32[47,128]{1,0:T(8,128)} %slice.1661) | copy-start | bytes 72196
  156.2 29.6 %copy-start.52 = (f32[47,128]{1,0:T(8,128)S(1)}, f32[47,128]{1,0:T(8,128)}, u32[]{:S(2)}) copy-start(f32[47,128]{1,0:T(8,128)} %slice.1664) | copy-start | bytes 72196
  156.2 29.7 %copy-start.132 = (f32[1,128]{1,0:T(1,128)S(1)}, f32[1,128]{1,0:T(1,128)}, u32[]{:S(2)}) copy-start(f32[1,128]{1,0:T(1,128)} %slice.1951) | copy-start | bytes 1540
  156.2 29.7 %copy-start.131 = (f32[1,128]{1,0:T(1,128)S(1)}, f32[1,128]{1,0:T(1,128)}, u32[]{:S(2)}) copy-start(f32[1,128]{1,0:T(1,128)} %slice.1930) | copy-start | bytes 1540
  156.2 29.8 %copy-start.134 = (f32[1,128]{1,0:T(1,128)S(1)}, f32[1,128]{1,0:T(1,128)}, u32[]{:S(2)}) copy-start(f32[1,128]{1,0:T(1,128)} %slice.1913) | copy-start | bytes 1540
  156.2 29.8 %copy-start.133 = (f32[1,128]{1,0:T(1,128)S(1)}, f32[1,128]{1,0:T(1,128)}, u32[]{:S(2)}) copy-start(f32[1,128]{1,0:T(1,128)} %slice.1892) | copy-start | bytes 1540
  179.4 6.8 %copy-start.18 = (f32[95,128]{1,0:T(8,128)S(1)}, f32[95,128]{1,0:T(8,128)}, u32[]{:S(2)}) copy-start(f32[95,128]{1,0:T(8,128)} %slice.1525) | copy-start | bytes 145924
  179.4 6.8 %copy-start.19 = (f32[95,128]{1,0:T(8,128)S(1)}, f32[95,128]{1,0:T(8,128)}, u32[]{:S(2)}) copy-start(f32[95,128]{1,0:T(8,128)} %slice.1586) | copy-start | bytes 145924
  187.5 4.6 %copy-start.64 = (f32[2,256]{1,0:T(2,128)S(1)}, f32[2,256]{1,0:T(2,128)}, u32[]{:S(2)}) copy-start(f32[2,256]{1,0:T(2,128)} %slice.1418) | copy-start | bytes 6148
  187.5 4.6 %copy-start.66 = (f32[2,256]{1,0:T(2,128)S(1)}, f32[2,256]{1,0:T(2,128)}, u32[]{:S(2)}) copy-start(f32[2,256]{1,0:T(2,128)} %slice.1438) | copy-start | bytes 6148
  187.5 4.6 %copy-start.83 = (f32[2,256]{1,0:T(2,128)S(1)}, f32[2,256]{1,0:T(2,128)}, u32[]{:S(2)}) copy-start(f32[2,256]{1,0:T(2,128)} %slice.1441) | copy-start | bytes 6148
  187.5 4.6 %copy-start.84 = (f32[2,256]{1,0:T(2,128)S(1)}, f32[2,256]{1,0:T(2,128)}, u32[]{:S(2)}) copy-start(f32[2,256]{1,0:T(2,128)} %slice.1445) | copy-start | bytes 6148
  187.5 4.6 %copy-start.112 = (f32[1,256]{1,0:T(1,128)S(1)}, f32[1,256]{1,0:T(1,128)}, u32[]{:S(2)}) copy-start(f32[1,256]{1,0:T(1,128)} %slice.1809) | copy-start | bytes 3076
  187.5 4.7 %copy-start.111 = (f32[1,256]{1,0:T(1,128)S(1)}, f32[1,256]{1,0:T(1,128)}, u32[]{:S(2)}) copy-start(f32[1,256]{1,0:T(1,128)} %slice.1792) | copy-start | bytes 3076
  187.5 4.7 %copy-start.53 = (f32[5,256]{1,0:T(8,128)S(1)}, f32[5,256]{1,0:T(8,128)}, u32[]{:S(2)}) copy-start(f32[5,256]{1,0:T(8,128)} %slice.1408) | copy-start | bytes 15364
  187.5 4.7 %copy-start.55 = (f32[5,256]{1,0:T(8,128)S(1)}, f32[5,256]{1,0:T(8,128)}, u32[]{:S(2)}) copy-start(f32[5,256]{1,0:T(8,128)} %slice.1443) | copy-start | bytes 15364
  187.5 4.7 %copy-start.61 = (f32[5,256]{1,0:T(8,128)S(1)}, f32[5,256]{1,0:T(8,128)}, u32[]{:S(2)}) copy-start(f32[5,256]{1,0:T(8,128)} %slice.1447) | copy-start | bytes 15364
  187.6 4.7 %copy-start.62 = (f32[5,256]{1,0:T(8,128)S(1)}, f32[5,256]{1,0:T(8,128)}, u32[]{:S(2)}) copy-start(f32[5,256]{1,0:T(8,128)} %slice.1451) | copy-start | bytes 15364
  187.6 4.7 %copy-start.110 = (f32[1,256]{1,0:T(1,128)S(1)}, f32[1,256]{1,0:T(1,128)}, u32[]{:S(2)}) copy-start(f32[1,256]{1,0:T(1,128)} %slice.1814) | copy-start | bytes 3076
  187.6 4.8 %copy-start.109 = (f32[1,256]{1,0:T(1,128)S(1)}, f32[1,256]{1,0:T(1,128)}, u32[]{:S(2)}) copy-start(f32[1,256]{1,0:T(1,128)} %slice.1791) | copy-start | bytes 3076
  187.6 4.8 %copy-start.44 = (f32[11,256]{1,0:T(8,128)S(1)}, f32[11,256]{1,0:T(8,128)}, u32[]{:S(2)}) copy-start(f32[11,256]{1,0:T(8,128)} %slice.1398) | copy-start | bytes 33796
  187.6 4.8 %copy-start.46 = (f32[11,256]{1,0:T(8,128)S(1)}, f32[11,256]{1,0:T(8,128)}, u32[]{:S(2)}) copy-start(f32[11,256]{1,0:T(8,128)} %slice.1449) | copy-start | bytes 33796
  187.6 4.8 %copy-start.57 = (f32[11,256]{1,0:T(8,128)S(1)}, f32[11,256]{1,0:T(8,128)}, u32[]{:S(2)}) copy-start(f32[11,256]{1,0:T(8,128)} %slice.1453) | copy-start | bytes 33796
  187.7 4.8 %copy-start.58 = (f32[11,256]{1,0:T(8,128)S(1)}, f32[11,256]{1,0:T(8,128)}, u32[]{:S(2)}) copy-start(f32[11,256]{1,0:T(8,128)} %slice.1457) | copy-start | bytes 33796
  188.4 4.2 copy-start.30
  188.5 4.3 copy-start.106
  201.9 19.9 %copy-start.69 = (f32[4,4]{0,1:T(4,128)S(1)}, f32[4,4]{0,1:T(4,128)}, u32[]{:S(2)}) copy-start(f32[4,4]{0,1:T(4,128)} %copy-done.68) | copy-start | bytes 196
  201.9 20.7 %copy-start.59 = (bf16[2,4,16,32]{3,2,1,0:T(8,128)(2,1)S(1)}, bf16[2,4,16,32]{3,2,1,0:T(8,128)(2,1)}, u32[]{:S(2)}) copy-start(bf16[2,4,16,32]{3,2,1,0:T(8,128)(2,1)} %param.25) | copy-start | bytes 24580
  203.7 34.8 %all-to-all-start = ((f32[64,8,256]{2,1,0:T(8,128)}), f32[64,8,256]{2,1,0:T(8,128)S(1)}, u32[]{:S(2)}, u32[]{:S(2)}) async-start(f32[64,8,256]{2,1,0:T(8,128)} %broadcast_in_dim.98), calls=%async_computation | async-start | bytes 1048576 | tf_op jit(solution)/shard_map/all_to_all | solution.py:11
  221.0 144.5 %all-gather.5.cloned.1.call-start = ((), (), s32[]{:S(2)}) async-start(), calls=%async_computation.7 | async-start | bytes 4259840 | tf_op jit(solution)/shard_map/all_gather | solution.py:180
  239.5 8.8 %copy-start.27 = (f32[64,1,256]{2,1,0:T(1,128)S(1)}, f32[64,1,256]{2,1,0:T(1,128)}, u32[]{:S(2)}) copy-start(f32[64,1,256]{2,1,0:T(1,128)} %get-tuple-element.47) | copy-start | bytes 196612
  239.5 8.8 %copy-start.28 = (f32[64,1,256]{2,1,0:T(1,128)S(1)}, f32[64,1,256]{2,1,0:T(1,128)}, u32[]{:S(2)}) copy-start(f32[64,1,256]{2,1,0:T(1,128)} %get-tuple-element.48) | copy-start | bytes 196612
  239.5 8.8 %copy-start.29 = (f32[64,1,256]{2,1,0:T(1,128)S(1)}, f32[64,1,256]{2,1,0:T(1,128)}, u32[]{:S(2)}) copy-start(f32[64,1,256]{2,1,0:T(1,128)} %get-tuple-element.49) | copy-start | bytes 196612
  240.8 56.1 %copy-start.5 = (f32[384,128]{1,0:T(8,128)S(1)}, f32[384,128]{1,0:T(8,128)}, u32[]{:S(2)}) copy-start(f32[384,128]{1,0:T(8,128)} %copy-done.4) | copy-start | bytes 589828
  250.3 48.2 %copy-start.1 = (f32[384,256]{1,0:T(8,128)S(1)}, f32[384,256]{1,0:T(8,128)}, u32[]{:S(2)}) copy-start(f32[384,256]{1,0:T(8,128)} %pad.434) | copy-start | bytes 1179652
  250.3 48.2 %copy-start.26 = (bf16[256,128]{0,1:T(8,128)(2,1)S(1)}, bf16[256,128]{0,1:T(8,128)(2,1)}, u32[]{:S(2)}) copy-start(bf16[256,128]{0,1:T(8,128)(2,1)} %reshape.352) | copy-start | bytes 196612
  300.7 12.6 %copy-start.122 = (f32[128]{0:T(128)S(1)}, f32[128]{0:T(128)}, u32[]{:S(2)}) copy-start(f32[128]{0:T(128)} %param.27) | copy-start | bytes 1540
  315.1 24.8 %all-to-all-start.2 = ((bf16[8,48,2048]{2,1,0:T(8,128)(2,1)}), bf16[8,48,2048]{2,1,0:T(8,128)(2,1)S(1)}, u32[]{:S(2)}, u32[]{:S(2)}) async-start(bf16[8,48,2048]{2,1,0:T(8,128)(2,1)} %bitcast.42), calls=%async_computation.2 | async-start | bytes 3145728 | tf_op jit(solution)/shard_map/all_to_all | solution.py:67
  319.3 22.0 %copy-start.82 = (f32[2048]{0:T(1024)S(1)}, f32[2048]{0:T(1024)}, u32[]{:S(2)}) copy-start(f32[2048]{0:T(1024)} %param.29) | copy-start | bytes 24580
  (93 other events, 230.8 us)
Sparse Core Ops, SparseCore 0:
  10.4 88.1 all-gather.2
  224.9 83.7 all-gather.4
where the time goes:
time: 438 us; the launch traced here: 431 us
  local copies, waits for them, and re-layouts  221 us (50%)
  blocking collectives  85 us (19%)
  other arithmetic  42.6 us (10%)
  waiting for transfers between devices  29.7 us (7%)
  starting transfers between devices  21.6 us (5%)
  between operations  17.3 us (4%)
  matrix products  13.5 us (3%)
    slice x224, local copies, waits for them, and re-layouts, kind_states(): lax.associative_scan(combine, (spike_magnitude * jnp.cos(angle)[None], sp...  146 us
    all_to_all x3, blocking collectives, copy_for_each(): lax.all_to_all(jnp.broadcast_to(value[None], (count, *value.shape)), axis...  59.9 us
    slice x80, local copies, waits for them, and re-layouts, joined_by_halves(): part[side::2]  47.9 us
    all_to_all x1, blocking collectives, sum_at_owner(): pieces = lax.all_to_all(split_up(value, dim, count), axis, 0, 0, tiled=True)  25.1 us
    all_to_all x1, waiting for transfers between devices, sum_at_owner(): pieces = lax.all_to_all(split_up(value, dim, count), axis, 0, 0, tiled=True)  20.6 us
    all_to_all x1, starting transfers between devices, copy_for_each(): lax.all_to_all(jnp.broadcast_to(value[None], (count, *value.shape)), axis...  17.3 us
    sub x13, other arithmetic, combine(): later[0] * earlier[0] - later[1] * earlier[1]  10.6 us
    concatenate x64, other arithmetic, kind_states(): lax.associative_scan(combine, (spike_magnitude * jnp.cos(angle)[None], sp...  10.2 us
  transfers between devices with their start and end apart: 4, of which 2 were waited for; matrix products, arithmetic and copies ran while one was open for 61% of the time, Pallas kernels for 0%

commit v1 on v0

v1 whole, which is shorter than its diff:
```python
import jax
import jax.numpy as jnp
from jax import lax
from jax.experimental import pallas as pl
from jax.experimental.pallas import tpu as pltpu
from jax.sharding import PartitionSpec as P

MESH = pl.DeviceIdType.MESH
BF, F32 = jnp.bfloat16, jnp.float32
EPS = 1e-06
NT = (((1,), (1,)), ((), ()))
STATES = 384
STEPS, LANES = 48, 8


def iota(shape, dim):
    return lax.broadcasted_iota(jnp.int32, shape, dim)


def one_row(values):
    rows, width = values.shape
    tiled = jnp.concatenate([values] * rows, axis=1)
    keep = iota(tiled.shape, 0) == iota(tiled.shape, 1) // width
    return jnp.sum(jnp.where(keep, tiled, 0.0), axis=0, keepdims=True)


def spread(column, width):
    rows = column.shape[0]
    shape = (rows, rows * width)
    keep = iota(shape, 0) == iota(shape, 1) // width
    return jnp.sum(jnp.where(keep, jnp.broadcast_to(column, shape), 0.0), axis=0, keepdims=True)


def expm1_small(x):
    total = jnp.ones_like(x)
    for order in range(9, 1, -1):
        total = 1.0 + total * x * (1.0 / order)
    return total * x


def times(a, b):
    return a[0] * b[0] - a[1] * b[1], a[0] * b[1] + a[1] * b[0]


def discretize(wide_poles, narrow_poles, log_step):
    real = jnp.concatenate([one_row(wide_poles[0]), one_row(narrow_poles[0])], axis=1)
    imag = jnp.concatenate([one_row(wide_poles[1]), one_row(narrow_poles[1])], axis=1)
    steps = log_step[...]
    step = jnp.exp(jnp.concatenate([spread(steps[:, :1], 64), spread(steps[:, 1:], 32)], axis=1))
    growth, angle = real * step, imag * step
    size, sine, cosine = jnp.exp(growth), jnp.sin(angle), jnp.cos(angle)
    half = jnp.sin(0.5 * angle)
    rise_real = expm1_small(growth) * cosine - 2.0 * half * half
    rise_imag = size * sine
    bottom = real * real + imag * imag
    coef_real = (rise_real * real + rise_imag * imag) / bottom
    coef_imag = (rise_imag * real - rise_real * imag) / bottom
    return (size * cosine, size * sine), (coef_real, coef_imag)


def in_blocks(wide_input, narrow_input):
    repeat = (iota((16, 128), 1) % 16 == iota((16, 128), 0)).astype(BF)
    out = []
    for part in range(2):
        for kind, (ref, width) in enumerate(((wide_input, 64), (narrow_input, 32))):
            flat = ref[part].reshape(4 * width, 16)
            tiled = jnp.dot(flat, repeat, preferred_element_type=F32)
            row, col = iota(tiled.shape, 0), iota(tiled.shape, 1)
            keep = (row // width == col // 32) & ((col // 16) % 2 == kind)
            out.append(jnp.where(keep, tiled, 0.0).astype(BF))
    return jnp.concatenate(out, axis=0)


def out_blocks(wide_output, narrow_output):
    out = []
    for part in range(2):
        halves = []
        for kind, (ref, width) in enumerate(((wide_output, 64), (narrow_output, 32))):
            flat = ref[part].reshape(64, width)
            row, col = iota((128, 64), 0), iota((128, 64), 1)
            pick = ((row // 32 == col // 16) & (row % 16 == col % 16)).astype(BF)
            rows = jnp.dot(pick, flat, preferred_element_type=F32).astype(BF)
            repeat = (iota((width, 4 * width), 1) % width == iota((width, 4 * width), 0)).astype(BF)
            tiled = jnp.dot(rows, repeat, preferred_element_type=F32)
            row, col = iota(tiled.shape, 0), iota(tiled.shape, 1)
            keep = (row // 32 == col // width) & ((row // 16) % 2 == kind)
            halves.append(jnp.where(keep, tiled, 0.0))
        whole = jnp.concatenate(halves, axis=1)
        out.append((whole if part == 0 else -whole).astype(BF))
    return out


def order():
    row, col = iota((384, 384), 0), iota((384, 384), 1)
    return (col == (row % LANES) * STEPS + row // LANES).astype(BF)


def back_order():
    row, col = iota((384, 384), 0), iota((384, 384), 1)
    return (row == (col % LANES) * STEPS + col // LANES).astype(BF)


def decay_rows(forget, pick):
    rows = jnp.concatenate([forget[p] for p in range(4)], axis=0)
    high = rows.astype(BF)
    rest = rows - high.astype(F32)
    middle = rest.astype(BF)
    low = (rest - middle.astype(F32)).astype(BF)
    parts = jnp.concatenate([high.astype(F32), middle.astype(F32), low.astype(F32)], axis=0).astype(BF)
    turned = lax.dot_general(pick, parts, NT, preferred_element_type=F32).astype(BF)
    row, col = iota((24, STATES), 0), iota((24, STATES), 1)
    group = jnp.where(col < 256, 2 * (col // 64), 2 * ((col - 256) // 32) + 1)
    place = (row % 8 == group).astype(BF)
    return jnp.exp(-jnp.dot(turned, place, preferred_element_type=F32))


def chain(first, ends, decay, run_base):
    now, starts = first, []
    for run in range(LANES):
        starts.append(now)
        part = slice(run, run + 1)
        grown = times(run_base, now)
        now = (
            decay[part] * grown[0] + ends[0][part],
            decay[part] * grown[1] + ends[1][part],
        )
    return [jnp.concatenate([s[i] for s in starts], axis=0) for i in range(2)], now


def kernel(
    hidden_in, drive, wide_poles, narrow_poles, log_step, forget, wide_input, narrow_input,
    wide_output, narrow_output, skip, mix_gain, out_weight, mlp_gain, up_weight, down_weight,
    out,
    up_a, up_b, dn_a, dn_b, mats, normed, part, final, own_in, carried, acc, pair_in, half_in, side_in,
    push_r, push_i, decay, ymsg, zmsg, gains, act_out, act_in, squared,
    loc_sem, s1_send, s1_recv, s2_send, s2_recv, y_send, y_recv, z_send, z_recv,
    g_send, g_recv, a_send, a_recv, ag_send, ag_recv, rs_send, rs_recv, out_sem,
):
    sp, tp = lax.axis_index("sp"), lax.axis_index("tp")
    y, z, x, core = sp % 8, sp // 8, tp // 2, tp % 2
    pending = []

    def along_y(step):
        return z * 8 + (y + step + 8) % 8, tp

    def along_z(step):
        return ((z + step + 8) % 8) * 8 + y, tp

    def group(step):
        return sp, (tp + step) % 8

    def along_x(step):
        return sp, ((x + step + 4) % 4) * 2 + core

    partner = (sp, 2 * x + 1 - core)

    def send(src, dst, send_sem, recv_sem, to):
        copy = pltpu.make_async_remote_copy(
            src_ref=src, dst_ref=dst, send_sem=send_sem, recv_sem=recv_sem, device_id=to, device_id_type=MESH
        )
        copy.start()
        pending.append(copy)

    def arrived(dst, recv_sem):
        pltpu.make_async_remote_copy(
            src_ref=dst, dst_ref=dst, send_sem=recv_sem, recv_sem=recv_sem, device_id=partner, device_id_type=MESH
        ).wait_recv()

    barrier = pltpu.get_barrier_semaphore()
    for step in range(1, 8):
        for to in (along_y(step), along_z(step), group(step)):
            pl.semaphore_signal(barrier, inc=1, device_id=to, device_id_type=MESH)
    bufs = (up_a, up_b, dn_a, dn_b)
    local = []
    for n, (weight, buf) in enumerate(zip((up_weight, up_weight, down_weight, down_weight), bufs)):
        local.append(
            pltpu.make_async_copy(weight.at[:, pl.ds((n % 2) * 512, 512)], buf.at[z, y], loc_sem.at[n])
        )
    local.append(pltpu.make_async_copy(out_weight, mats.at[tp], loc_sem.at[4]))
    local.append(pltpu.make_async_copy(hidden_in.at[pl.ds(pl.multiple_of(tp * 48, 16), 48)], own_in, loc_sem.at[5]))
    for copy in local:
        copy.start()
    for copy in local:
        copy.wait()
    pl.semaphore_wait(barrier, 21)

    def shard(n, first, second):
        return bufs[n].at[second, first] if n % 2 == 0 else bufs[n].at[first, second]

    def pair(n, q, second):
        both = pl.ds(2 * q, 2)
        return bufs[n].at[second, both] if n % 2 == 0 else bufs[n].at[both, second]

    def where_of(n):
        return (y, z, along_y, along_z) if n % 2 == 0 else (z, y, along_z, along_y)

    def mod8(v):
        return (v + 8) % 8

    def first_send(n, direction, hop):
        at, line, go, _ = where_of(n)
        k = (0 if direction > 0 else 4) + hop - 1
        ref = shard(n, mod8(at - direction * (hop - 1)), line)
        send(ref, ref, s1_send.at[n, k], s1_recv.at[n, k], go(direction))

    def first_wait(n, direction, hop):
        at, line, _, _ = where_of(n)
        k = (0 if direction > 0 else 4) + hop - 1
        arrived(shard(n, mod8(at - direction * hop), line), s1_recv.at[n, k])

    def first_start(n):
        first_send(n, 1, 1)
        first_send(n, -1, 1)

    def first_step(n, hop):
        first_wait(n, 1, hop)
        if hop < 4:
            first_send(n, 1, hop + 1)
            first_wait(n, -1, hop)
            if hop < 3:
                first_send(n, -1, hop + 1)

    def pair_at(n, r):
        at = where_of(n)[0]
        lean = 2 * (at % 2) - 1
        return (at // 2 + (0, lean, -lean, 2)[r] + 4) % 4

    def line_key(direction, hop, r):
        return (0 if direction > 0 else 16) + (hop - 1) * 4 + r

    def line_send(n, direction, hop, r):
        _, line, _, go = where_of(n)
        k = line_key(direction, hop, r)
        ref = pair(n, pair_at(n, r), mod8(line - direction * (hop - 1)))
        send(ref, ref, s2_send.at[n, k], s2_recv.at[n, k], go(direction))

    def line_wait(n, direction, hop, r):
        _, line, _, _ = where_of(n)
        k = line_key(direction, hop, r)
        arrived(pair(n, pair_at(n, r), mod8(line - direction * hop)), s2_recv.at[n, k])

    def line_start(ns, r):
        for n in ns:
            line_send(n, 1, 1, r)
            line_send(n, -1, 1, r)

    def line_step(ns, hop, r):
        for n in ns:
            for direction in (1, -1):
                last = r < 2 if direction > 0 else r >= 2
                if hop < 4 or last:
                    line_wait(n, direction, hop, r)
                    if hop < 3 or (hop == 3 and last):
                        line_send(n, direction, hop + 1, r)

    ups, downs = (0, 1), (2, 3)

    halves = (pl.ds(0, 1024), pl.ds(1024, 1024))

    def gather_start(buf, g):
        ref = buf.at[tp]
        send(ref, ref, ag_send.at[g, 0], ag_recv.at[g, 0], along_x(1))
        send(ref, ref, ag_send.at[g, 1], ag_recv.at[g, 1], along_x(-1))
        send(ref, ref, ag_send.at[g, 2], ag_recv.at[g, 2], partner)

    def gather_middle(buf, g):
        for n, direction in enumerate((1, -1)):
            ref = buf.at[along_x(-direction)[1]]
            arrived(ref, ag_recv.at[g, n])
            piece = ref.at[:, halves[n]]
            send(piece, piece, ag_send.at[g, 3 + n], ag_recv.at[g, 3 + n], along_x(direction))
            send(ref, ref, ag_send.at[g, 5 + n], ag_recv.at[g, 5 + n], partner)

    def gather_end(buf, g):
        far = buf.at[along_x(2)[1]]
        for n in range(2):
            piece = far.at[:, halves[n]]
            arrived(piece, ag_recv.at[g, 3 + n])
            send(piece, piece, ag_send.at[g, 7 + n], ag_recv.at[g, 7 + n], partner)

    def gather_partner(buf, g):
        def theirs(step):
            return buf.at[((x + step + 4) % 4) * 2 + 1 - core]

        arrived(theirs(0), ag_recv.at[g, 2])
        for n, direction in enumerate((1, -1)):
            arrived(theirs(-direction), ag_recv.at[g, 5 + n])
        for n in range(2):
            arrived(theirs(2).at[:, halves[n]], ag_recv.at[g, 7 + n])

    for n in range(4):
        first_start(n)
    gather_start(mats, 0)
    gains[tp] = mix_gain[...]
    for step in range(1, 8):
        send(mix_gain, gains.at[tp], g_send.at[step], g_recv.at[tp], group(step))

    pick = order()
    decay[...] = decay_rows(forget, pick)
    drive_now = jnp.dot(pick, drive[...], preferred_element_type=F32).astype(BF)
    for n in range(4):
        first_step(n, 1)
    line_start(ups, 0)
    base, coef = discretize(wide_poles, narrow_poles, log_step)
    pushed = lax.dot_general(drive_now, in_blocks(wide_input, narrow_input), NT, preferred_element_type=F32)
    pushed = times(coef, (pushed[:, :STATES], pushed[:, STATES:]))
    push_r[...] = pushed[0]
    push_i[...] = pushed[1]
    for n in range(4):
        first_step(n, 2)
    line_start(ups, 1)
    wide_base = [jnp.broadcast_to(b, (LANES, STATES)) for b in base]

    def scan_step(step, state):
        rows = pl.ds(pl.multiple_of(step * LANES, LANES), LANES)
        fade = decay[rows]
        grown = times(wide_base, state[:2])
        new = fade * grown[0] + push_r[rows], fade * grown[1] + push_i[rows], fade * state[2]
        push_r[rows], push_i[rows], decay[rows] = new
        return new

    zero = jnp.zeros((LANES, STATES), F32)
    end_r, end_i, total = lax.fori_loop(0, STEPS, scan_step, (zero, zero, zero + 1.0), unroll=4)
    powers = [base]
    for _ in range(5):
        powers.append(times(powers[-1], powers[-1]))
    run_base = times(powers[5], powers[4])
    _, last = chain((zero[:1], zero[:1]), (end_r, end_i), total, run_base)
    fade_all = total[:1]
    for run in range(1, LANES):
        fade_all = fade_all * total[run : run + 1]
    device_base = run_base
    for _ in range(3):
        device_base = times(device_base, device_base)
    line_base = device_base
    for _ in range(3):
        line_base = times(line_base, line_base)

    def message(buf, at, state, fade):
        buf[at] = jnp.concatenate([state[0], state[1], fade, jnp.zeros((5, STATES), F32)], axis=0)

    message(ymsg, y, last, fade_all)
    for step in range(1, 8):
        send(ymsg.at[y], ymsg.at[y], y_send.at[step], y_recv.at[y], along_y(step))
    for n in range(4):
        first_step(n, 3)
    line_start(ups, 2)
    for step in range(1, 8):
        arrived(ymsg.at[(y + step) % 8], y_recv.at[(y + step) % 8])
    zrow, onerow = zero[:1], zero[:1] + 1.0
    whole, before = (zrow, zrow), (zrow, zrow)
    whole_fade, before_fade, before_base = onerow, onerow, (onerow, zrow)
    for k in range(8):
        got = ymsg[k]
        fade = got[2:3]
        grown = times(device_base, whole)
        new = fade * grown[0] + got[0:1], fade * grown[1] + got[1:2]
        new_fade = whole_fade * fade
        new_base = times(before_base, device_base)
        earlier = k < y
        before = [jnp.where(earlier, n, o) for n, o in zip(new, before)]
        before_fade = jnp.where(earlier, new_fade, before_fade)
        before_base = [jnp.where(earlier, n, o) for n, o in zip(new_base, before_base)]
        whole, whole_fade = new, new_fade
    message(zmsg, z, whole, whole_fade)
    for step in range(1, 8):
        send(zmsg.at[z], zmsg.at[z], z_send.at[step], z_recv.at[z], along_z(step))
    for n in range(4):
        first_step(n, 4)
    line_start(ups, 3)
    for r in range(4):
        line_step(ups, 1, r)
    for step in range(1, 8):
        arrived(zmsg.at[(z + step) % 8], z_recv.at[(z + step) % 8])
    enter = (zrow, zrow)
    for k in range(8):
        got = zmsg[k]
        grown = times(line_base, enter)
        new = got[2:3] * grown[0] + got[0:1], got[2:3] * grown[1] + got[1:2]
        enter = [jnp.where(k < z, n, o) for n, o in zip(new, enter)]
    grown = times(before_base, enter)
    enter = before_fade * grown[0] + before[0], before_fade * grown[1] + before[1]
    starts, _ = chain(enter, (end_r, end_i), total, run_base)

    def fix_step(step, state):
        rows = pl.ds(pl.multiple_of(step * LANES, LANES), LANES)
        state = times(wide_base, state)
        push_r[rows] = push_r[rows] + decay[rows] * state[0]
        push_i[rows] = push_i[rows] + decay[rows] * state[1]
        return state

    lax.fori_loop(0, STEPS, fix_step, tuple(starts), unroll=4)
    real_block, imag_block = out_blocks(wide_output, narrow_output)
    response = lax.dot_general(push_r[...].astype(BF), real_block, NT, preferred_element_type=F32)
    response += lax.dot_general(push_i[...].astype(BF), imag_block, NT, preferred_element_type=F32)
    response += skip[...] * drive_now.astype(F32)
    active = 0.5 * response * (1.0 + lax.erf(response * (0.5**0.5)))
    active = jnp.dot(back_order(), active.astype(BF), preferred_element_type=F32).astype(BF)
    act_out[...] = active.reshape(8, 48, 128)
    act_in[tp] = act_out[tp]
    for step in range(1, 8):
        to = group(step)
        send(act_out.at[to[1]], act_in.at[tp], a_send.at[step], a_recv.at[tp], to)
    for r in range(4):
        line_step(ups, 2, r)
        line_start(downs, r)
    gather_middle(mats, 0)
    for step in range(1, 8):
        source = (tp + step) % 8
        arrived(gains.at[source], g_recv.at[source])
        arrived(act_in.at[source], a_recv.at[source])
    rows = jnp.concatenate([act_in[k] for k in range(8)], axis=1).astype(F32)
    gain = jnp.concatenate([gains[k] for k in range(8)], axis=1)
    power = jnp.sum(rows * rows, axis=1, keepdims=True) * (1.0 / 1024)
    mixed = (rows * lax.rsqrt(power + EPS) * gain).astype(BF)
    for r in range(4):
        line_step(ups, 3, r)
    gather_end(mats, 0)
    gather_partner(mats, 0)
    for n in range(8):
        cols = pl.ds(n * 256, 256)
        proj = jnp.dot(mixed, mats[:, :, cols].reshape(1024, 256), preferred_element_type=F32)
        carried[:, cols] = (own_in[:, cols].astype(F32) + proj).astype(BF)
    values = carried[...].astype(F32)
    power = jnp.sum(values * values, axis=1, keepdims=True) * (1.0 / 2048)
    normed[tp] = (values * lax.rsqrt(power + EPS) * mlp_gain[...]).astype(BF)
    gather_start(normed, 1)
    for r in range(4):
        line_step(ups, 4, r)
        line_step(downs, 1, r)
    gather_middle(normed, 1)
    for r in range(4):
        line_step(downs, 2, r)
    gather_end(normed, 1)
    gather_partner(normed, 1)

    for n in range(4):
        cols = pl.ds((n % 2) * 256, 256)
        pre = jnp.dot(
            normed[...].reshape(384, 2048),
            bufs[n // 2][:, :, :, cols].reshape(2048, 256),
            preferred_element_type=F32,
        )
        pre = jnp.maximum(pre, 0.0)
        squared[:, pl.ds(n * 256, 256)] = (pre * pre).astype(BF)
    for r in range(4):
        line_step(downs, 3, r)
    for r in range(4):
        line_step(downs, 4, r)
    for n in range(8):
        piece = lax.dot_general(squared[:, :512], dn_a[n].reshape(256, 512), NT, preferred_element_type=F32)
        piece += lax.dot_general(squared[:, 512:], dn_b[n].reshape(256, 512), NT, preferred_element_type=F32)
        part[:, :, :, pl.ds(n * 256, 256)] = piece.astype(BF).reshape(4, 2, 48, 256)

    def chip(step):
        return (x + step + 4) % 4

    for n, step in enumerate((2, 1, -1, 0)):
        to = chip(step)
        send(part.at[to, 1 - core], pair_in.at[to], rs_send.at[n], rs_recv.at[n], partner)

    def both(step, n):
        arrived(pair_in.at[chip(step)], rs_recv.at[n])
        return part[chip(step), core].astype(F32) + pair_in[chip(step)].astype(F32)

    acc[0] = both(2, 0).astype(BF)
    send(acc.at[0, :, halves[0]], half_in.at[0], rs_send.at[4], rs_recv.at[4], along_x(1))
    send(acc.at[0, :, halves[1]], half_in.at[1], rs_send.at[5], rs_recv.at[5], along_x(-1))
    right = both(1, 1)
    acc[1, :, 1024:] = right[:, 1024:].astype(BF)
    send(acc.at[1, :, halves[1]], side_in.at[0, :, halves[1]], rs_send.at[6], rs_recv.at[6], along_x(1))
    left = both(-1, 2)
    acc[2, :, :1024] = left[:, :1024].astype(BF)
    send(acc.at[2, :, halves[0]], side_in.at[1, :, halves[0]], rs_send.at[7], rs_recv.at[7], along_x(-1))
    arrived(half_in.at[0], rs_recv.at[4])
    acc[1, :, :1024] = (right[:, :1024] + half_in[0].astype(F32)).astype(BF)
    send(acc.at[1, :, halves[0]], side_in.at[0, :, halves[0]], rs_send.at[8], rs_recv.at[8], along_x(1))
    arrived(half_in.at[1], rs_recv.at[5])
    acc[2, :, 1024:] = (left[:, 1024:] + half_in[1].astype(F32)).astype(BF)
    send(acc.at[2, :, halves[1]], side_in.at[1, :, halves[1]], rs_send.at[9], rs_recv.at[9], along_x(-1))
    mine = both(0, 3) + carried[...].astype(F32)
    for copy in pending[:-13]:
        copy.wait_send()
    del pending[:-13]
    arrived(side_in.at[0, :, halves[1]], rs_recv.at[6])
    arrived(side_in.at[1, :, halves[0]], rs_recv.at[7])
    arrived(side_in.at[0, :, halves[0]], rs_recv.at[8])
    arrived(side_in.at[1, :, halves[1]], rs_recv.at[9])
    final[tp] = (mine + side_in[0].astype(F32) + side_in[1].astype(F32)).astype(BF)

    gather_start(final, 2)
    gather_middle(final, 2)
    gather_end(final, 2)
    gather_partner(final, 2)
    copy = pltpu.make_async_copy(final, out, out_sem)
    copy.start()
    for sent in pending:
        sent.wait_send()
    copy.wait()


def step(*args):
    args = list(args)
    for n in (10, 11, 13):
        args[n] = args[n].reshape(1, -1)
    vmem, hbm = pl.BlockSpec(memory_space=pltpu.VMEM), pl.BlockSpec(memory_space=pl.ANY)
    dma = pltpu.SemaphoreType.DMA
    scratch = [
        *[pltpu.VMEM((8, 8, 32, 512), BF)] * 4,
        pltpu.VMEM((8, 128, 2048), BF),
        pltpu.VMEM((8, 48, 2048), BF),
        pltpu.VMEM((4, 2, 48, 2048), BF),
        pltpu.VMEM((8, 48, 2048), BF),
        pltpu.VMEM((48, 2048), BF),
        pltpu.VMEM((48, 2048), BF),
        pltpu.VMEM((3, 48, 2048), BF),
        pltpu.VMEM((4, 48, 2048), BF),
        pltpu.VMEM((2, 48, 1024), BF),
        pltpu.VMEM((2, 48, 2048), BF),
        *[pltpu.VMEM((384, STATES), F32)] * 3,
        *[pltpu.VMEM((8, 8, STATES), F32)] * 2,
        pltpu.VMEM((8, 1, 128), F32),
        pltpu.VMEM((8, 48, 128), BF),
        pltpu.VMEM((8, 48, 128), BF),
        pltpu.VMEM((384, 1024), BF),
        dma((6,)), dma((4, 7)), dma((4, 7)), dma((4, 32)), dma((4, 32)),
        *[dma((8,))] * 8,
        dma((3, 9)), dma((3, 9)), dma((10,)), dma((10,)), dma,
    ]
    whole = pl.pallas_call(
        kernel,
        out_shape=jax.ShapeDtypeStruct((8, 48, 2048), BF),
        in_specs=[hbm if n in (0, 12, 14, 15) else vmem for n in range(16)],
        out_specs=hbm,
        scratch_shapes=scratch,
        compiler_params=pltpu.CompilerParams(
            collective_id=0, has_side_effects=True, vmem_limit_bytes=60 * 1024 * 1024
        ),
    )(*args)
    return whole.reshape(384, 2048)


def solution(mesh):
    return jax.shard_map(
        step,
        mesh=mesh,
        in_specs=(
            P("sp", None),
            P("sp", "tp"),
            P(None, "tp", None),
            P(None, "tp", None),
            P("tp", None),
            P("tp", None, "sp"),
            P(None, "tp", None, None),
            P(None, "tp", None, None),
            P(None, "tp", None, None),
            P(None, "tp", None, None),
            P("tp"),
            P("tp"),
            P("tp", None),
            P(),
            P("sp", "tp"),
            P("sp", "tp"),
        ),
        out_specs=P("sp", None),
        check_vma=False,
    )
```

time: 438 us -> 108 us (0.25); the launches traced: 431 us -> 107 us
  local copies, waits for them, and re-layouts: 221 us -> 7.05 us
  Pallas kernels: 0 us -> 99.5 us
  blocking collectives: 85 us -> 0 us
  other arithmetic: 42.6 us -> 0 us
  waiting for transfers between devices: 29.7 us -> 0 us
  starting transfers between devices: 21.6 us -> 0 us
  between operations: 17.3 us -> 0.01 us
  matrix products: 13.5 us -> 0 us
    slice x308 -> x0, local copies, waits for them, and re-layouts: 197 us -> none  [the longest x224 146 us: kind_states(): lax.associative_scan(combine, (spike_magnitude * jnp.cos(angle)[None], sp...]
    pallas_call x0 -> x1, Pallas kernels: none -> 99.5 us  [step(): pl.pallas_call(kernel, out_shape=jax.ShapeDtypeStruct((8, 48, 2048), BF),...]
    all_to_all x4 -> x0, blocking collectives: 85 us -> none  [the longest x3 59.9 us: copy_for_each(): lax.all_to_all(jnp.broadcast_to(value[None], (count, *value.shape)), axis...]
    all_to_all x2 -> x0, waiting for transfers between devices: 28.3 us -> none  [the longest x1 20.6 us: sum_at_owner(): pieces = lax.all_to_all(split_up(value, dim, count), axis, 0, 0, tiled=True)]
    all_to_all x2 -> x0, starting transfers between devices: 21.5 us -> none  [the longest x1 17.3 us: copy_for_each(): lax.all_to_all(jnp.broadcast_to(value[None], (count, *value.shape)), axis...]
    add x107 -> x0, other arithmetic: 15.4 us -> none  [the longest x24 7.59 us: combine(): later[0] * earlier[3] + later[1] * earlier[2] + later[3]]
    dot_general x10 -> x0, matrix products: 13.5 us -> none  [the longest x1 8.02 us: local(): lax.dot_general(squared, down_whole, (((1,), (1,)), ((), ())), preferred_...]
    sub x13 -> x0, other arithmetic: 10.6 us -> none  [combine(): later[0] * earlier[0] - later[1] * earlier[1]]
  transfers between devices with their start and end apart: 4 -> 0, of which waited for: 2 -> 0; matrix products, arithmetic and copies ran while one was open for 61% -> 0% of each run, Pallas kernels for 0% -> 0%
where the time goes in v1:
time: 108 us; the launch traced here: 107 us
  Pallas kernels  99.5 us (92%)
  local copies, waits for them, and re-layouts  7.05 us (7%)
    pallas_call x1, Pallas kernels, step(): pl.pallas_call(kernel, out_shape=jax.ShapeDtypeStruct((8, 48, 2048), BF),...  99.5 us
    unnamed x4, local copies, waits for them, and re-layouts  7.05 us

profile of v1, /device:TPU:1, one launch (start us, length us, event | category | flops | bytes accessed | tf_op | source)
XLA Modules:
  0.0 106.6 jit_solution(3299867329753464580)
XLA Ops:
  0.0 1.3 %copy.17.log_step = f32[4,2]{1,0:T(4,128)} copy(f32[4,2]{0,1:T(2,128)} %param.20) | data formatting | bytes 64 | tf_op args[4]
  1.3 1.5 %copy.19.narrow_input = bf16[2,4,32,16]{3,2,1,0:T(8,128)(2,1)} copy(bf16[2,4,32,16]{2,3,1,0:T(8,128)(2,1)} %param.23) | data formatting | bytes 16384 | tf_op args[7]
  2.8 1.5 %copy.18.wide_input = bf16[2,4,64,16]{3,2,1,0:T(8,128)(2,1)} copy(bf16[2,4,64,16]{2,3,1,0:T(8,128)(2,1)} %param.22) | data formatting | bytes 32768 | tf_op args[6]
  4.3 99.5 %shard_map.154 = bf16[8,48,2048]{2,1,0:T(8,128)(2,1)} custom-call(bf16[384,2048]{1,0:T(8,128)(2,1)} %hidden_in.1, bf16[384,128]{1,0:T(8,128)(2,1)} %drive.1, f32[2,4,64]{2,1,0:T(4,128)} %wide_poles.1, f32[2,4,32]{2,1,0:T(4,128)} %narrow_poles.1, f32[4,2]{1,0:T(4,128)} %copy.17.log_step, f32[4,2,384]{2,1,0:T(2,128)} %forget.1, ...), custom_call_target="tpu_custom_call" | custom-call | tf_op jit(solution)/shard_map/pallas_call | solution.py:530
  103.8 2.7 %copy.21 = bf16[384,2048]{1,0:T(8,128)(2,1)} copy(bf16[384,2048]{1,0:T(8,128)(2,1)} %bitcast.4) | data formatting | bytes 3145728

commit v2 on v1

v2 whole, which is shorter than its diff:
```python
import jax
import jax.numpy as jnp
from jax import lax
from jax.experimental import pallas as pl
from jax.experimental.pallas import tpu as pltpu
from jax.sharding import PartitionSpec as P

MESH = pl.DeviceIdType.MESH
BF, F32 = jnp.bfloat16, jnp.float32
EPS = 1e-06
NT = (((1,), (1,)), ((), ()))
STATES = 384
STEPS, LANES = 48, 8


def iota(shape, dim):
    return lax.broadcasted_iota(jnp.int32, shape, dim)


def one_row(values):
    rows, width = values.shape
    tiled = jnp.concatenate([values] * rows, axis=1)
    keep = iota(tiled.shape, 0) == iota(tiled.shape, 1) // width
    return jnp.sum(jnp.where(keep, tiled, 0.0), axis=0, keepdims=True)


def spread(line, width):
    keep = iota((4, 4), 0) == iota((4, 4), 1)
    column = jnp.sum(jnp.where(keep, jnp.broadcast_to(line, (4, 4)), 0.0), axis=1, keepdims=True)
    shape = (4, 4 * width)
    keep = iota(shape, 0) == iota(shape, 1) // width
    return jnp.sum(jnp.where(keep, jnp.broadcast_to(column, shape), 0.0), axis=0, keepdims=True)


def expm1_small(x):
    total = jnp.ones_like(x)
    for order in range(9, 1, -1):
        total = 1.0 + total * x * (1.0 / order)
    return total * x


def times(a, b):
    return a[0] * b[0] - a[1] * b[1], a[0] * b[1] + a[1] * b[0]


def discretize(wide_poles, narrow_poles, log_step):
    real = jnp.concatenate([one_row(wide_poles[0]), one_row(narrow_poles[0])], axis=1)
    imag = jnp.concatenate([one_row(wide_poles[1]), one_row(narrow_poles[1])], axis=1)
    steps = log_step[...]
    step = jnp.exp(jnp.concatenate([spread(steps[:1], 64), spread(steps[1:], 32)], axis=1))
    growth, angle = real * step, imag * step
    size, sine, cosine = jnp.exp(growth), jnp.sin(angle), jnp.cos(angle)
    half = jnp.sin(0.5 * angle)
    rise_real = expm1_small(growth) * cosine - 2.0 * half * half
    rise_imag = size * sine
    bottom = real * real + imag * imag
    coef_real = (rise_real * real + rise_imag * imag) / bottom
    coef_imag = (rise_imag * real - rise_real * imag) / bottom
    return (size * cosine, size * sine), (coef_real, coef_imag)


def blocks(first, second):
    out = []
    for part in range(2):
        halves = []
        for kind, (ref, width) in enumerate(((first, 64), (second, 32))):
            flat = ref[part].reshape(64, width)
            row, col = iota((128, 64), 0), iota((128, 64), 1)
            pick = ((row // 32 == col // 16) & (row % 16 == col % 16)).astype(BF)
            rows = jnp.dot(pick, flat, preferred_element_type=F32).astype(BF)
            repeat = (iota((width, 4 * width), 1) % width == iota((width, 4 * width), 0)).astype(BF)
            tiled = jnp.dot(rows, repeat, preferred_element_type=F32)
            row, col = iota(tiled.shape, 0), iota(tiled.shape, 1)
            keep = (row // 32 == col // width) & ((row // 16) % 2 == kind)
            halves.append(jnp.where(keep, tiled, 0.0))
        out.append(jnp.concatenate(halves, axis=1))
    return out


def order():
    row, col = iota((384, 384), 0), iota((384, 384), 1)
    return (col == (row % LANES) * STEPS + row // LANES).astype(BF)


def back_order():
    row, col = iota((384, 384), 0), iota((384, 384), 1)
    return (row == (col % LANES) * STEPS + col // LANES).astype(BF)


def decay_rows(forget, pick):
    rows = jnp.concatenate([forget[p] for p in range(4)], axis=0)
    high = rows.astype(BF)
    rest = rows - high.astype(F32)
    middle = rest.astype(BF)
    low = (rest - middle.astype(F32)).astype(BF)
    parts = jnp.concatenate([high.astype(F32), middle.astype(F32), low.astype(F32)], axis=0).astype(BF)
    turned = lax.dot_general(pick, parts, NT, preferred_element_type=F32).astype(BF)
    row, col = iota((24, STATES), 0), iota((24, STATES), 1)
    group = jnp.where(col < 256, 2 * (col // 64), 2 * ((col - 256) // 32) + 1)
    place = (row % 8 == group).astype(BF)
    return jnp.exp(-jnp.dot(turned, place, preferred_element_type=F32))


def chain(first, ends, decay, run_base):
    now, starts = first, []
    for run in range(LANES):
        starts.append(now)
        part = slice(run, run + 1)
        grown = times(run_base, now)
        now = (
            decay[part] * grown[0] + ends[0][part],
            decay[part] * grown[1] + ends[1][part],
        )
    return [jnp.concatenate([s[i] for s in starts], axis=0) for i in range(2)], now


def kernel(
    hidden_in, drive, wide_poles, narrow_poles, log_step, forget, wide_input, narrow_input,
    wide_output, narrow_output, skip, mix_gain, out_weight, mlp_gain, up_weight, down_weight,
    out,
    up_a, up_b, dn_a, dn_b, mats, normed, part, own_in, carried, acc, pair_in, half_in, side_in,
    push_r, push_i, decay, ymsg, zmsg, gains, act_out, act_in, squared,
    loc_sem, w_send, s1_recv, s2_recv, m_send, m_recv, ag_send, ag_recv, t_send, t_recv,
):
    sp, tp = lax.axis_index("sp"), lax.axis_index("tp")
    y, z, x, core = sp % 8, sp // 8, tp // 2, tp % 2

    def along_y(step):
        return z * 8 + (y + step + 8) % 8, tp

    def along_z(step):
        return ((z + step + 8) % 8) * 8 + y, tp

    def group(step):
        return sp, (tp + step) % 8

    def along_x(step):
        return sp, ((x + step + 4) % 4) * 2 + core

    partner = (sp, 2 * x + 1 - core)

    def send(src, dst, send_sem, recv_sem, to):
        pltpu.make_async_remote_copy(
            src_ref=src, dst_ref=dst, send_sem=send_sem, recv_sem=recv_sem, device_id=to, device_id_type=MESH
        ).start()

    def held(ref, sem):
        return pltpu.make_async_remote_copy(
            src_ref=ref, dst_ref=ref, send_sem=sem, recv_sem=sem, device_id=partner, device_id_type=MESH
        )

    def arrived(dst, recv_sem):
        held(dst, recv_sem).wait_recv()

    def left(src, send_sem):
        held(src, send_sem).wait_send()

    barrier = pltpu.get_barrier_semaphore()
    for step in range(1, 8):
        for to in (along_y(step), along_z(step), group(step)):
            pl.semaphore_signal(barrier, inc=1, device_id=to, device_id_type=MESH)
    bufs = (up_a, up_b, dn_a, dn_b)

    def where_of(n):
        return (y, z, along_y, along_z) if n % 2 == 0 else (z, y, along_z, along_y)

    def shard(n, first, second):
        return bufs[n].at[second * 8 + first]

    def pair(n, q, second):
        return bufs[n].at[pl.ds(second * 8 + 2 * q, 2)]

    def mod8(v):
        return (v + 8) % 8

    local = []
    for n, weight in enumerate((up_weight, up_weight, down_weight, down_weight)):
        at, line, _, _ = where_of(n)
        local.append(
            pltpu.make_async_copy(weight.at[:, pl.ds((n % 2) * 512, 512)], shard(n, at, line), loc_sem.at[n])
        )
    local.append(pltpu.make_async_copy(out_weight, mats.at[tp], loc_sem.at[4]))
    local.append(pltpu.make_async_copy(hidden_in.at[pl.ds(pl.multiple_of(tp * 48, 16), 48)], own_in, loc_sem.at[5]))
    for copy in local:
        copy.start()
    def first_key(direction, hop):
        return (0 if direction > 0 else 4) + hop - 1

    def direct_start(n):
        at, line, go, _ = where_of(n)
        ref = shard(n, at, line)
        for hop in range(1, 5):
            for direction in (1, -1) if hop < 4 else (1,):
                send(ref, ref, w_send.at[n], s1_recv.at[n, first_key(direction, hop)], go(direction * hop))

    def first_send(n, direction, hop):
        at, line, go, _ = where_of(n)
        ref = shard(n, mod8(at - direction * (hop - 1)), line)
        send(ref, ref, w_send.at[n], s1_recv.at[n, first_key(direction, hop)], go(direction))

    def first_wait(n, direction, hop):
        at, line, _, _ = where_of(n)
        arrived(shard(n, mod8(at - direction * hop), line), s1_recv.at[n, first_key(direction, hop)])

    def direct_wait(n, hop):
        first_wait(n, 1, hop)
        if hop < 4:
            first_wait(n, -1, hop)

    def first_step(n, hop):
        first_wait(n, 1, hop)
        if hop < 4:
            first_send(n, 1, hop + 1)
            first_wait(n, -1, hop)
            if hop < 3:
                first_send(n, -1, hop + 1)

    def pair_at(n, r):
        at = where_of(n)[0]
        lean = 2 * (at % 2) - 1
        return (at // 2 + (0, lean, -lean, 2)[r] + 4) % 4

    def line_key(direction, hop, r):
        if hop == 4:
            return 24 + r
        return (0 if direction > 0 else 12) + (hop - 1) * 4 + r

    def line_send(n, direction, hop, r):
        _, line, _, go = where_of(n)
        ref = pair(n, pair_at(n, r), mod8(line - direction * (hop - 1)))
        send(ref, ref, w_send.at[n], s2_recv.at[n, line_key(direction, hop, r)], go(direction))

    def line_wait(n, direction, hop, r):
        _, line, _, _ = where_of(n)
        arrived(pair(n, pair_at(n, r), mod8(line - direction * hop)), s2_recv.at[n, line_key(direction, hop, r)])

    def line_start(ns, r):
        for n in ns:
            line_send(n, 1, 1, r)
            line_send(n, -1, 1, r)

    def line_step(ns, hop, r):
        for n in ns:
            for direction in (1, -1):
                last = r < 2 if direction > 0 else r >= 2
                if hop < 4 or last:
                    line_wait(n, direction, hop, r)
                    if hop < 3 or (hop == 3 and last):
                        line_send(n, direction, hop + 1, r)

    ups, downs = (0, 1), (2, 3)

    halves = (pl.ds(0, 1024), pl.ds(1024, 1024))

    def gather_start(buf, g):
        ref = buf.at[tp]
        for turn in range(2):
            for n, direction in enumerate((1, -1)):
                half = (n + turn) % 2
                piece = ref.at[:, halves[half]]
                send(piece, piece, ag_send.at[g], ag_recv.at[g, 2 * n + turn], along_x(direction))
        send(ref, ref, ag_send.at[g], ag_recv.at[g, 6], partner)

    def gather_middle(buf, g, turns=(0, 1)):
        for turn in turns:
            for n, direction in enumerate((1, -1)):
                half = (n + turn) % 2
                piece = buf.at[along_x(-direction)[1], :, halves[half]]
                arrived(piece, ag_recv.at[g, 2 * n + turn])
                if turn == 0:
                    send(piece, piece, ag_send.at[g], ag_recv.at[g, 4 + n], along_x(direction))
                send(piece, piece, ag_send.at[g], ag_recv.at[g, 6], partner)

    def gather_end(buf, g):
        far = buf.at[along_x(2)[1]]
        for n in range(2):
            piece = far.at[:, halves[n]]
            arrived(piece, ag_recv.at[g, 4 + n])
            send(piece, piece, ag_send.at[g], ag_recv.at[g, 6], partner)

    def gather_partner(buf, g):
        arrived(buf.at[pl.ds(0, 4)], ag_recv.at[g, 6])

    def message(buf, at, state, fade):
        buf[at] = jnp.concatenate([state[0], state[1], fade, fade], axis=0)

    pick = order()
    decay[...] = decay_rows(forget, pick)
    drive_now = jnp.dot(pick, drive[...], preferred_element_type=F32).astype(BF)
    base, coef = discretize(wide_poles, narrow_poles, log_step)
    weights = [b.astype(BF) for b in blocks(wide_input, narrow_input)]
    pushed = times(coef, [jnp.dot(drive_now, w, preferred_element_type=F32) for w in weights])
    push_r[...] = pushed[0]
    push_i[...] = pushed[1]
    wide_base = [jnp.broadcast_to(b, (LANES, STATES)) for b in base]

    def scan_step(step, state):
        rows = pl.ds(pl.multiple_of(step * LANES, LANES), LANES)
        fade = decay[rows]
        grown = times(wide_base, state[:2])
        new = fade * grown[0] + push_r[rows], fade * grown[1] + push_i[rows], fade * state[2]
        push_r[rows], push_i[rows], decay[rows] = new
        return new

    zero = jnp.zeros((LANES, STATES), F32)
    end_r, end_i, total = lax.fori_loop(0, STEPS, scan_step, (zero, zero, zero + 1.0), unroll=4)
    powers = [base]
    for _ in range(5):
        powers.append(times(powers[-1], powers[-1]))
    run_base = times(powers[5], powers[4])
    _, last = chain((zero[:1], zero[:1]), (end_r, end_i), total, run_base)
    fade_all = total[:1]
    for run in range(1, LANES):
        fade_all = fade_all * total[run : run + 1]
    device_base = run_base
    for _ in range(3):
        device_base = times(device_base, device_base)
    line_base = device_base
    for _ in range(3):
        line_base = times(line_base, line_base)

    for copy in local:
        copy.wait()
    pl.semaphore_wait(barrier, 21)

    message(ymsg, y, last, fade_all)
    for step in range(1, 8):
        send(ymsg.at[y], ymsg.at[y], m_send.at[1], m_recv.at[1], along_y(step))
    for n in range(4):
        first_send(n, 1, 1)
        first_send(n, -1, 1)
    gather_start(mats, 0)
    gains[tp] = mix_gain[...]
    for step in range(1, 8):
        send(mix_gain, gains.at[tp], m_send.at[0], m_recv.at[0], group(step))
    for n in range(4):
        first_step(n, 1)
    line_start(ups, 0)
    arrived(ymsg.at[pl.ds(0, 7)], m_recv.at[1])
    zrow, onerow = zero[:1], zero[:1] + 1.0
    whole, before = (zrow, zrow), (zrow, zrow)
    whole_fade, before_fade, before_base = onerow, onerow, (onerow, zrow)
    for k in range(8):
        got = ymsg[k]
        fade = got[2:3]
        grown = times(device_base, whole)
        new = fade * grown[0] + got[0:1], fade * grown[1] + got[1:2]
        new_fade = whole_fade * fade
        new_base = times(before_base, device_base)
        earlier = k < y
        before = [jnp.where(earlier, n, o) for n, o in zip(new, before)]
        before_fade = jnp.where(earlier, new_fade, before_fade)
        before_base = [jnp.where(earlier, n, o) for n, o in zip(new_base, before_base)]
        whole, whole_fade = new, new_fade
    message(zmsg, z, whole, whole_fade)
    for step in range(1, 8):
        send(zmsg.at[z], zmsg.at[z], m_send.at[2], m_recv.at[2], along_z(step))
    for n in range(4):
        first_step(n, 2)
    line_start(ups, 1)
    line_step(ups, 1, 0)
    for n in range(4):
        first_step(n, 3)
    line_start(ups, 2)
    arrived(zmsg.at[pl.ds(0, 7)], m_recv.at[2])
    enter = (zrow, zrow)
    for k in range(8):
        got = zmsg[k]
        grown = times(line_base, enter)
        new = got[2:3] * grown[0] + got[0:1], got[2:3] * grown[1] + got[1:2]
        enter = [jnp.where(k < z, n, o) for n, o in zip(new, enter)]
    grown = times(before_base, enter)
    enter = before_fade * grown[0] + before[0], before_fade * grown[1] + before[1]
    line_step(ups, 1, 1)
    for n in range(4):
        first_step(n, 4)
    line_start(ups, 3)
    starts, _ = chain(enter, (end_r, end_i), total, run_base)

    def fix_step(step, state):
        rows = pl.ds(pl.multiple_of(step * LANES, LANES), LANES)
        state = times(wide_base, state)
        push_r[rows] = push_r[rows] + decay[rows] * state[0]
        push_i[rows] = push_i[rows] + decay[rows] * state[1]
        return state

    lax.fori_loop(0, STEPS, fix_step, tuple(starts), unroll=4)
    real_block, imag_block = blocks(wide_output, narrow_output)
    response = lax.dot_general(push_r[...].astype(BF), real_block.astype(BF), NT, preferred_element_type=F32)
    response -= lax.dot_general(push_i[...].astype(BF), imag_block.astype(BF), NT, preferred_element_type=F32)
    response += skip[...] * drive_now.astype(F32)
    active = 0.5 * response * (1.0 + lax.erf(response * (0.5**0.5)))
    active = jnp.dot(back_order(), active.astype(BF), preferred_element_type=F32).astype(BF)
    act_out[...] = active.reshape(8, 48, 128)
    act_in[tp] = act_out[tp]
    for step in range(1, 8):
        to = group(step)
        send(act_out.at[to[1]], act_in.at[tp], m_send.at[3], m_recv.at[3], to)
    line_step(ups, 2, 0)
    line_step(ups, 1, 2)
    line_step(ups, 2, 1)
    line_step(ups, 1, 3)
    gather_middle(mats, 0, (0,))
    line_start(downs, 0)
    line_step(ups, 2, 2)
    line_start(downs, 1)
    arrived(gains.at[pl.ds(0, 7)], m_recv.at[0])
    arrived(act_in.at[pl.ds(0, 7)], m_recv.at[3])
    rows = jnp.concatenate([act_in[k] for k in range(8)], axis=1).astype(F32)
    gain = jnp.concatenate([gains[k] for k in range(8)], axis=1)
    power = jnp.sum(rows * rows, axis=1, keepdims=True) * (1.0 / 1024)
    mixed = (rows * lax.rsqrt(power + EPS) * gain).astype(BF)
    line_step(ups, 2, 3)
    gather_middle(mats, 0, (1,))
    line_step(ups, 3, 0)
    line_start((2,), 2)
    line_step(ups, 3, 1)
    line_start((2,), 3)
    gather_end(mats, 0)
    gather_partner(mats, 0)
    for n in range(8):
        cols = pl.ds(n * 256, 256)
        proj = jnp.dot(mixed, mats[:, :, cols].reshape(1024, 256), preferred_element_type=F32)
        carried[:, cols] = (own_in[:, cols].astype(F32) + proj).astype(BF)
    values = carried[...].astype(F32)
    power = jnp.sum(values * values, axis=1, keepdims=True) * (1.0 / 2048)
    normed[tp] = (values * lax.rsqrt(power + EPS) * mlp_gain[...]).astype(BF)
    gather_start(normed, 1)
    def down_at(pos):
        line_step((2,), pos // 4 + 1, pos % 4)
        line_step((3,), pos % 8 // 2 + 1, pos % 2 + 2 * (pos // 8))

    line_step(ups, 3, 2)
    line_step(ups, 3, 3)
    down_at(0)
    line_step(ups, 4, 0)
    line_step(ups, 4, 1)
    gather_middle(normed, 1, (0,))
    line_step(ups, 4, 2)
    line_step(ups, 4, 3)
    down_at(1)
    gather_middle(normed, 1, (1,))
    down_at(2)
    gather_end(normed, 1)
    down_at(3)
    gather_partner(normed, 1)

    for n in range(4):
        cols = pl.ds((n % 2) * 256, 256)
        buf = bufs[n // 2]
        if n < 2:
            weight = buf[:, :, cols].reshape(2048, 256)
        else:
            weight = jnp.concatenate([buf[(s % 8) * 8 + s // 8, :, cols] for s in range(64)], axis=0)
        pre = jnp.dot(normed[...].reshape(384, 2048), weight, preferred_element_type=F32)
        pre = jnp.maximum(pre, 0.0)
        squared[:, pl.ds(n * 256, 256)] = (pre * pre).astype(BF)

    def chip(step):
        return (x + step + 4) % 4

    small = (pl.ds(0, 256), pl.ds(256, 256))

    def columns(r, half=None):
        start = pair_at(3, r) * 512
        if half is None:
            return pl.ds(pl.multiple_of(start, 512), 512)
        return pl.ds(pl.multiple_of(start + half * 256, 256), 256)

    def product(r):
        q = pair_at(3, r)
        first = dn_a[pl.ds(pl.multiple_of(q * 16, 16), 16)].reshape(512, 512)
        second = jnp.concatenate([dn_b[(s % 8) * 8 + 2 * q + s // 8] for s in range(16)], axis=0)
        piece = lax.dot_general(squared[:, :512], first, NT, preferred_element_type=F32)
        piece += lax.dot_general(squared[:, 512:], second, NT, preferred_element_type=F32)
        piece = piece.astype(BF)
        for b in range(8):
            part[r * 8 + (b % 2) * 4 + b // 2] = piece[b * 48 : (b + 1) * 48]
        send(part.at[pl.ds(r * 8 + (1 - core) * 4, 4)], pair_in.at[r], t_send.at[r], t_recv.at[r, 0], partner)

    def chip_sum(r, step):
        return part[r * 8 + core * 4 + chip(step)].astype(F32) + pair_in[r, chip(step)].astype(F32)

    def sums_out(r):
        arrived(pair_in.at[r], t_recv.at[r, 0])
        acc[r, 0] = chip_sum(r, 2).astype(BF)
        for n, direction in enumerate((1, -1)):
            send(acc.at[r, 0, :, small[n]], half_in.at[r, n], t_send.at[r], t_recv.at[r, 1 + n], along_x(direction))
        for n, direction in enumerate((1, -1)):
            acc[r, 1 + n] = chip_sum(r, direction).astype(BF)
            ready = small[1 - n]
            send(
                acc.at[r, 1 + n, :, ready], side_in.at[r, n, :, ready],
                t_send.at[r], t_recv.at[r, 3], along_x(direction),
            )

    def sums_on(r):
        for n, direction in enumerate((1, -1)):
            arrived(half_in.at[r, n], t_recv.at[r, 1 + n])
            cols = slice(n * 256, (n + 1) * 256)
            acc[r, 1 + n, :, cols] = (chip_sum(r, direction)[:, cols] + half_in[r, n].astype(F32)).astype(BF)
            send(
                acc.at[r, 1 + n, :, small[n]], side_in.at[r, n, :, small[n]],
                t_send.at[r], t_recv.at[r, 3], along_x(direction),
            )

    def finish(r):
        mine = chip_sum(r, 0) + carried[:, columns(r)].astype(F32)
        arrived(side_in.at[r], t_recv.at[r, 3])
        out[tp, :, columns(r)] = (mine + side_in[r, 0].astype(F32) + side_in[r, 1].astype(F32)).astype(BF)
        ref = out.at[tp, :, columns(r)]
        for n, direction in enumerate((1, -1)):
            send(ref, ref, t_send.at[r], t_recv.at[r, 4 + n], along_x(direction))
        send(ref, ref, t_send.at[r], t_recv.at[r, 8], partner)

    def pass_on(r):
        for n, direction in enumerate((1, -1)):
            at = along_x(-direction)[1]
            arrived(out.at[at, :, columns(r)], t_recv.at[r, 4 + n])
            piece = out.at[at, :, columns(r, n)]
            send(piece, piece, t_send.at[r], t_recv.at[r, 6 + n], along_x(direction))
            ref = out.at[at, :, columns(r)]
            send(ref, ref, t_send.at[r], t_recv.at[r, 8], partner)

    def pass_last(r):
        for n in range(2):
            piece = out.at[along_x(2)[1], :, columns(r, n)]
            arrived(piece, t_recv.at[r, 6 + n])
            send(piece, piece, t_send.at[r], t_recv.at[r, 8], partner)

    for pos in range(4, 7):
        down_at(pos)
    line_start((3,), 2)
    line_start((3,), 3)
    product(0)
    down_at(7)
    product(1)
    sums_out(0)
    down_at(8)
    sums_out(1)
    down_at(9)
    sums_on(0)
    down_at(10)
    sums_on(1)
    finish(0)
    down_at(11)
    finish(1)
    down_at(12)
    pass_on(0)
    down_at(13)
    pass_on(1)
    down_at(14)
    pass_last(0)
    down_at(15)
    product(2)
    product(3)
    pass_last(1)
    for n in range(4):
        left(bufs[n].at[pl.ds(0, 63)], w_send.at[n])
    left(gains.at[pl.ds(0, 7)], m_send.at[0])
    left(ymsg.at[pl.ds(0, 7)], m_send.at[1])
    left(zmsg.at[pl.ds(0, 7)], m_send.at[2])
    left(act_out.at[pl.ds(0, 7)], m_send.at[3])
    left(mats.at[pl.ds(0, 7)], ag_send.at[0])
    left(normed.at[pl.ds(0, 7)], ag_send.at[1])
    for r in (2, 3):
        sums_out(r)
    for r in (2, 3):
        sums_on(r)
    for r in (2, 3):
        finish(r)
    for r in (2, 3):
        pass_on(r)
    for r in (2, 3):
        pass_last(r)
    for r in range(4):
        arrived(part.at[pl.ds(0, 4)], t_recv.at[r, 8])
    for r in range(4):
        left(part.at[pl.ds(0, 14)], t_send.at[r])


def step(*args):
    args = list(args)
    for n in (10, 11, 13):
        args[n] = args[n].reshape(1, -1)
    args[4] = args[4].T
    for n in (6, 7):
        args[n] = jnp.swapaxes(args[n], 2, 3)
    vmem, hbm = pl.BlockSpec(memory_space=pltpu.VMEM), pl.BlockSpec(memory_space=pltpu.HBM)
    dma = pltpu.SemaphoreType.DMA
    scratch = [
        *[pltpu.VMEM((64, 32, 512), BF)] * 4,
        pltpu.VMEM((8, 128, 2048), BF),
        pltpu.VMEM((8, 48, 2048), BF),
        pltpu.VMEM((32, 48, 512), BF),
        pltpu.VMEM((48, 2048), BF),
        pltpu.VMEM((48, 2048), BF),
        pltpu.VMEM((4, 3, 48, 512), BF),
        pltpu.VMEM((4, 4, 48, 512), BF),
        pltpu.VMEM((4, 2, 48, 256), BF),
        pltpu.VMEM((4, 2, 48, 512), BF),
        *[pltpu.VMEM((384, STATES), F32)] * 3,
        *[pltpu.VMEM((8, 4, STATES), F32)] * 2,
        pltpu.VMEM((8, 1, 128), F32),
        pltpu.VMEM((8, 48, 128), BF),
        pltpu.VMEM((8, 48, 128), BF),
        pltpu.VMEM((384, 1024), BF),
        dma((6,)), dma((4,)), dma((4, 7)), dma((4, 28)), dma((4,)), dma((4,)),
        dma((2,)), dma((2, 7)), dma((4,)), dma((4, 9)),
    ]
    whole = pl.pallas_call(
        kernel,
        out_shape=jax.ShapeDtypeStruct((8, 48, 2048), BF),
        in_specs=[hbm if n in (0, 12, 14, 15) else vmem for n in range(16)],
        out_specs=vmem,
        scratch_shapes=scratch,
        compiler_params=pltpu.CompilerParams(
            collective_id=0, has_side_effects=True, vmem_limit_bytes=58 * 1024 * 1024
        ),
    )(*args)
    return whole.reshape(384, 2048)


def solution(mesh):
    return jax.shard_map(
        step,
        mesh=mesh,
        in_specs=(
            P("sp", None),
            P("sp", "tp"),
            P(None, "tp", None),
            P(None, "tp", None),
            P("tp", None),
            P("tp", None, "sp"),
            P(None, "tp", None, None),
            P(None, "tp", None, None),
            P(None, "tp", None, None),
            P(None, "tp", None, None),
            P("tp"),
            P("tp"),
            P("tp", None),
            P(),
            P("sp", "tp"),
            P("sp", "tp"),
        ),
        out_specs=P("sp", None),
        check_vma=False,
    )
```

time: 108 us -> 102 us (0.944); the launches traced: 107 us -> 102 us
  local copies, waits for them, and re-layouts: 7.05 us -> 2.73 us
    unnamed x4 -> x1, local copies, waits for them, and re-layouts: 7.05 us -> 2.73 us
where the time goes in v2:
time: 102 us
  Pallas kernels  99.4 us (97%)
  local copies, waits for them, and re-layouts  2.73 us (3%)
    pallas_call x1, Pallas kernels, step(): pl.pallas_call(kernel, out_shape=jax.ShapeDtypeStruct((8, 48, 2048), BF),...  99.4 us
    unnamed x1, local copies, waits for them, and re-layouts  2.73 us

profile of v2, /device:TPU:1, one launch (start us, length us, event | category | flops | bytes accessed | tf_op | source)
XLA Modules:
  0.0 102.1 jit_solution(8100476484805074742)
XLA Ops:
  0.0 99.4 %shard_map.154 = bf16[8,48,2048]{2,1,0:T(8,128)(2,1)} custom-call(bf16[384,2048]{1,0:T(8,128)(2,1)} %hidden_in.1, bf16[384,128]{1,0:T(8,128)(2,1)} %drive.1, f32[2,4,64]{2,1,0:T(4,128)} %wide_poles.1, f32[2,4,32]{2,1,0:T(4,128)} %narrow_poles.1, f32[2,4]{1,0:T(2,128)} %bitcast.11, f32[4,2,384]{2,1,0:T(2,128)} %forget.1, bf16[2,4,16,64]{3,2,1,0:T(8,128)(2,1)} %bitcast.8, ...), custom_call_target="tpu_custom_call" | custom-call | tf_op jit(solution)/shard_map/pallas_call | solution.py:611
  99.4 2.7 %copy.18 = bf16[384,2048]{1,0:T(8,128)(2,1)} copy(bf16[384,2048]{1,0:T(8,128)(2,1)} %bitcast.7) | data formatting | bytes 3145728

commit v3 on v2

v3 whole, which is shorter than its diff:
```python
import jax
import jax.numpy as jnp
from jax import lax
from jax.experimental import pallas as pl
from jax.experimental.pallas import tpu as pltpu
from jax.sharding import PartitionSpec as P

MESH = pl.DeviceIdType.MESH
BF, F32 = jnp.bfloat16, jnp.float32
EPS = 1e-06
NT = (((1,), (1,)), ((), ()))
STATES = 384
STEPS, LANES = 48, 8


def iota(shape, dim):
    return lax.broadcasted_iota(jnp.int32, shape, dim)


def one_row(values):
    rows, width = values.shape
    tiled = jnp.concatenate([values] * rows, axis=1)
    keep = iota(tiled.shape, 0) == iota(tiled.shape, 1) // width
    return jnp.sum(jnp.where(keep, tiled, 0.0), axis=0, keepdims=True)


def spread(line, width):
    keep = iota((4, 4), 0) == iota((4, 4), 1)
    column = jnp.sum(jnp.where(keep, jnp.broadcast_to(line, (4, 4)), 0.0), axis=1, keepdims=True)
    shape = (4, 4 * width)
    keep = iota(shape, 0) == iota(shape, 1) // width
    return jnp.sum(jnp.where(keep, jnp.broadcast_to(column, shape), 0.0), axis=0, keepdims=True)


def expm1_small(x):
    total = jnp.ones_like(x)
    for order in range(9, 1, -1):
        total = 1.0 + total * x * (1.0 / order)
    return total * x


def times(a, b):
    return a[0] * b[0] - a[1] * b[1], a[0] * b[1] + a[1] * b[0]


def discretize(wide_poles, narrow_poles, log_step):
    real = jnp.concatenate([one_row(wide_poles[0]), one_row(narrow_poles[0])], axis=1)
    imag = jnp.concatenate([one_row(wide_poles[1]), one_row(narrow_poles[1])], axis=1)
    steps = log_step[...]
    step = jnp.exp(jnp.concatenate([spread(steps[:1], 64), spread(steps[1:], 32)], axis=1))
    growth, angle = real * step, imag * step
    size, sine, cosine = jnp.exp(growth), jnp.sin(angle), jnp.cos(angle)
    half = jnp.sin(0.5 * angle)
    rise_real = expm1_small(growth) * cosine - 2.0 * half * half
    rise_imag = size * sine
    bottom = real * real + imag * imag
    coef_real = (rise_real * real + rise_imag * imag) / bottom
    coef_imag = (rise_imag * real - rise_real * imag) / bottom
    return (size * cosine, size * sine), (coef_real, coef_imag)


def blocks(first, second):
    out = []
    for part in range(2):
        halves = []
        for kind, (ref, width) in enumerate(((first, 64), (second, 32))):
            flat = ref[part].reshape(64, width)
            row, col = iota((128, 64), 0), iota((128, 64), 1)
            pick = ((row // 32 == col // 16) & (row % 16 == col % 16)).astype(BF)
            rows = jnp.dot(pick, flat, preferred_element_type=F32).astype(BF)
            repeat = (iota((width, 4 * width), 1) % width == iota((width, 4 * width), 0)).astype(BF)
            tiled = jnp.dot(rows, repeat, preferred_element_type=F32)
            row, col = iota(tiled.shape, 0), iota(tiled.shape, 1)
            keep = (row // 32 == col // width) & ((row // 16) % 2 == kind)
            halves.append(jnp.where(keep, tiled, 0.0))
        out.append(jnp.concatenate(halves, axis=1))
    return out


def order():
    row, col = iota((384, 384), 0), iota((384, 384), 1)
    return (col == (row % LANES) * STEPS + row // LANES).astype(BF)


def back_order():
    row, col = iota((384, 384), 0), iota((384, 384), 1)
    return (row == (col % LANES) * STEPS + col // LANES).astype(BF)


def decay_rows(forget, pick):
    rows = jnp.concatenate([forget[p] for p in range(4)], axis=0)
    high = rows.astype(BF)
    rest = rows - high.astype(F32)
    middle = rest.astype(BF)
    low = (rest - middle.astype(F32)).astype(BF)
    parts = jnp.concatenate([high.astype(F32), middle.astype(F32), low.astype(F32)], axis=0).astype(BF)
    turned = lax.dot_general(pick, parts, NT, preferred_element_type=F32).astype(BF)
    row, col = iota((24, STATES), 0), iota((24, STATES), 1)
    group = jnp.where(col < 256, 2 * (col // 64), 2 * ((col - 256) // 32) + 1)
    place = (row % 8 == group).astype(BF)
    return jnp.exp(-jnp.dot(turned, place, preferred_element_type=F32))


def chain(first, ends, decay, run_base):
    now, starts = first, []
    for run in range(LANES):
        starts.append(now)
        part = slice(run, run + 1)
        grown = times(run_base, now)
        now = (
            decay[part] * grown[0] + ends[0][part],
            decay[part] * grown[1] + ends[1][part],
        )
    return [jnp.concatenate([s[i] for s in starts], axis=0) for i in range(2)], now


OFFSETS = (0, -1, 1, -2, 2, -3, 3, 4)
RIGHTWARD = (0, 1, 4, 5)
CHUNKS = ((0, 1, 2), (3, 4), (5, 6), (7,))
DIRECT = (2, 3)
COPY, DELAY, ISSUE, AHEAD = 0.703, 2.2, 0.03, 2.5
DUE = (32.0, 36.0, 42.0, 46.0)


def chunk_of(s):
    return [n for n, chunk in enumerate(CHUNKS) if s in chunk][0]


def slack(op):
    kind, n, s, hop = op
    step = DELAY + COPY
    if kind == "first":
        return (0.0 if n < 2 else 8.0) + hop
    if n < 2:
        return 15.0 - (4 - hop) * step
    if n == 3:
        return DUE[chunk_of(s)] - (4 - hop) * step
    return min(DUE[h - 1] - (h - hop) * step for h in range(hop, 5))


def waits_of(n, chunk=None):
    ops = []
    if chunk is None or chunk == 0:
        ops += [("first", n, 0, hop) for hop in range(1, 5)]
    for s in range(8):
        for hop in range(1, 5):
            mine = chunk is None or (hop == chunk + 1 if n == 2 else chunk_of(s) == chunk)
            if mine:
                ops.append(("line", n, s, hop))
    return set(ops)


def steps_of():
    ups = waits_of(0) | waits_of(1)
    steps = {
        "ywait": ((), 4.3, 0.1, set()),
        "zwait": (("ywait",), 4.5, 0.1, set()),
        "readout": (("zwait",), 0.0, 1.3, set()),
        "mats0": ((), 8.5, 0.05, set()),
        "mats1": (("mats0",), 5.6, 0.05, set()),
        "act": (("readout", "mats1"), 3.5, 0.2, set()),
        "mats2": (("mats1",), 5.0, 0.05, set()),
        "proj": (("act", "mats2"), 1.3, 1.0, set()),
        "rows0": (("proj",), 4.3, 0.05, set()),
        "rows1": (("rows0",), 2.1, 0.05, set()),
        "rows2": (("rows1",), 2.1, 0.05, set()),
        "up": (("rows2",), 1.3, 1.8, ups),
    }
    for c, chunk in enumerate(CHUNKS):
        width = len(chunk)
        needs = waits_of(2, c) | waits_of(3, c)
        steps[f"product{c}"] = (("up",) if c == 0 else ("up", f"product{c - 1}"), 0.0, 0.35 * width, needs)
        steps[f"sum{c}"] = ((f"product{c}",), 1.3 + 0.2 * width, 0.1, set())
        final = c in DIRECT
        if not final:
            steps[f"on{c}"] = ((f"sum{c}",), 2.4 + 0.5 * width, 0.1, set())
        steps[f"done{c}"] = ((f"sum{c}" if final else f"on{c}",), (3.2 + 1.0 * width) if final else 2.8 + 0.5 * width, 0.1, set())
        steps[f"pass{c}"] = ((f"done{c}",), 3.2 + 1.0 * width if final else 2.8 + 0.5 * width, 0.05, set())
        if not final:
            steps[f"last{c}"] = ((f"pass{c}",), 2.4 + 0.3 * width, 0.05, set())
        steps[f"out{c}"] = ((f"pass{c}" if final else f"last{c}",), 1.2, 0.05, set())
    steps["clean"] = ((f"product{len(CHUNKS) - 1}",), 0.1, 0.2, set())
    return steps


def plan():
    steps, order = steps_of(), []
    free, ready, coming = [1.0, 0.0], [set(), set()], []
    ended, seen, now = {}, set(), 0.0

    def link(op):
        return (op[1] + (op[0] == "line")) % 2

    def offer(op):
        ready[link(op)].add(op)

    for n in range(4):
        offer(("first", n, 0, 1))
        offer(("line", n, 0, 1))
    while steps or coming or ready[0] or ready[1]:
        for side in range(2):
            ahead = AHEAD
            for name, (before, after, own, needs) in steps.items():
                if own > 0.9 and all(b in ended for b in before) and needs <= seen:
                    if max([ended[b] for b in before], default=0.0) + after < now + 0.3:
                        ahead = AHEAD + own
            while ready[side] and free[side] - now < ahead:
                op = min(ready[side], key=lambda o: (slack(o), o))
                ready[side].remove(op)
                order.append(("send", op))
                both = 1.0 if op[3] < 4 else 0.5
                free[side] = max(free[side], now) + COPY * both
                coming.append((free[side] + DELAY, op))
                now += ISSUE
        due = min(coming, default=None)
        able = [
            (max([ended[b] for b in before], default=0.0) + after, name)
            for name, (before, after, _, needs) in steps.items()
            if all(b in ended for b in before) and needs <= seen
        ]
        step = min(able, default=None)
        if due and due[0] <= now or (due and (step is None or due[0] < step[0])):
            now = max(now, due[0]) + ISSUE
            coming.remove(due)
            op = due[1]
            seen.add(op)
            order.append(("wait", op))
            kind, n, s, hop = op
            if hop < 4:
                offer((kind, n, s, hop + 1))
            if kind == "first":
                for k, offset in enumerate(OFFSETS):
                    if abs(offset) == hop:
                        offer(("line", n, k, 1))
        elif step:
            wake = [free[side] - AHEAD * 0.5 for side in range(2) if ready[side]]
            if wake and min(wake) < step[0] and min(wake) > now:
                now = min(wake)
                continue
            now = max(now, step[0]) + steps[step[1]][2]
            ended[step[1]] = now
            order.append(("step", step[1]))
            if step[1] == "ywait":
                free[1] = max(free[1], now) + 1.0
            del steps[step[1]]
        else:
            now = max(now, min(free[side] for side in range(2) if ready[side]) - AHEAD * 0.5)
    return order, ended, now


def kernel(
    hidden_in, drive, wide_poles, narrow_poles, log_step, forget, wide_input, narrow_input,
    wide_output, narrow_output, skip, mix_gain, out_weight, mlp_gain, up_weight, down_weight,
    out,
    up_a, up_b, dn_a, dn_b, mats, normed, own_in, carried,
    push_r, push_i, decay, ymsg, zmsg, gains, act_out, act_in, squared,
    loc_sem, w_send, s1_recv, s2_recv, m_send, m_recv, ag_send, ag_recv, t_send, t_recv, out_sem,
    *pieces,
):
    part, pair_in, acc, half_in, side_in, final = (pieces[n :: 6] for n in range(6))
    sp, tp = lax.axis_index("sp"), lax.axis_index("tp")
    y, z, x, core = sp % 8, sp // 8, tp // 2, tp % 2

    def along_y(step):
        return z * 8 + (y + step + 8) % 8, tp

    def along_z(step):
        return ((z + step + 8) % 8) * 8 + y, tp

    def group(step):
        return sp, (tp + step) % 8

    def along_x(step):
        return sp, ((x + step + 4) % 4) * 2 + core

    partner = (sp, 2 * x + 1 - core)

    def send(src, dst, send_sem, recv_sem, to):
        pltpu.make_async_remote_copy(
            src_ref=src, dst_ref=dst, send_sem=send_sem, recv_sem=recv_sem, device_id=to, device_id_type=MESH
        ).start()

    def held(ref, sem):
        return pltpu.make_async_remote_copy(
            src_ref=ref, dst_ref=ref, send_sem=sem, recv_sem=sem, device_id=partner, device_id_type=MESH
        )

    def arrived(dst, recv_sem):
        held(dst, recv_sem).wait_recv()

    def left(src, send_sem):
        held(src, send_sem).wait_send()

    barrier = pltpu.get_barrier_semaphore()
    for step in range(1, 8):
        for to in (along_y(step), along_z(step), group(step)):
            pl.semaphore_signal(barrier, inc=1, device_id=to, device_id_type=MESH)
    bufs = (up_a, up_b, dn_a, dn_b)

    def where_of(n):
        return (y, z, along_y, along_z) if n % 2 == 0 else (z, y, along_z, along_y)

    def shard(n, first, second):
        return bufs[n].at[second * 8 + first]

    def mod8(v):
        return (v + 8) % 8

    local = []
    for n, weight in enumerate((up_weight, up_weight, down_weight, down_weight)):
        at, line, _, _ = where_of(n)
        local.append(
            pltpu.make_async_copy(weight.at[:, pl.ds((n % 2) * 512, 512)], shard(n, at, line), loc_sem.at[n])
        )
    local.append(pltpu.make_async_copy(out_weight, mats.at[tp], loc_sem.at[4]))
    local.append(pltpu.make_async_copy(hidden_in.at[pl.ds(pl.multiple_of(tp * 48, 16), 48)], own_in, loc_sem.at[5]))
    for copy in local:
        copy.start()
    def first_send(n, hop):
        at, line, go, _ = where_of(n)
        for direction in (1, -1) if hop < 4 else (1,):
            ref = shard(n, mod8(at - direction * (hop - 1)), line)
            send(ref, ref, w_send.at[n], s1_recv.at[n, hop - 1], go(direction))

    def line_send(n, s, hop):
        at, line, _, go = where_of(n)
        for direction in (1, -1):
            if hop < 4 or (s in RIGHTWARD) == (direction > 0):
                ref = shard(n, mod8(at + OFFSETS[s]), mod8(line - direction * (hop - 1)))
                send(ref, ref, w_send.at[n], s2_recv.at[n, 4 * s + hop - 1], go(direction))

    def copy_send(op):
        kind, n, s, hop = op
        if kind == "first":
            first_send(n, hop)
        else:
            line_send(n, s, hop)

    def copy_wait(op):
        kind, n, s, hop = op
        sem = s1_recv.at[n, hop - 1] if kind == "first" else s2_recv.at[n, 4 * s + hop - 1]
        arrived(bufs[n].at[pl.ds(0, 2 if hop < 4 else 1)], sem)

    halves = (pl.ds(0, 1024), pl.ds(1024, 1024))

    def gather_start(buf, g):
        ref = buf.at[tp]
        for turn in range(2):
            for n, direction in enumerate((1, -1)):
                half = (n + turn) % 2
                piece = ref.at[:, halves[half]]
                send(piece, piece, ag_send.at[g], ag_recv.at[g, 2 * n + turn], along_x(direction))
        send(ref, ref, ag_send.at[g], ag_recv.at[g, 6], partner)

    def gather_middle(buf, g, turns=(0, 1)):
        for turn in turns:
            for n, direction in enumerate((1, -1)):
                half = (n + turn) % 2
                piece = buf.at[along_x(-direction)[1], :, halves[half]]
                arrived(piece, ag_recv.at[g, 2 * n + turn])
                if turn == 0:
                    send(piece, piece, ag_send.at[g], ag_recv.at[g, 4 + n], along_x(direction))
                send(piece, piece, ag_send.at[g], ag_recv.at[g, 6], partner)

    def gather_end(buf, g):
        far = buf.at[along_x(2)[1]]
        for n in range(2):
            piece = far.at[:, halves[n]]
            arrived(piece, ag_recv.at[g, 4 + n])
            send(piece, piece, ag_send.at[g], ag_recv.at[g, 6], partner)

    def gather_partner(buf, g):
        arrived(buf.at[pl.ds(0, 4)], ag_recv.at[g, 6])

    def message(buf, at, state, fade):
        buf[at] = jnp.concatenate([state[0], state[1], fade, fade], axis=0)

    pick = order()
    decay[...] = decay_rows(forget, pick)
    drive_now = jnp.dot(pick, drive[...], preferred_element_type=F32).astype(BF)
    base, coef = discretize(wide_poles, narrow_poles, log_step)
    weights = [b.astype(BF) for b in blocks(wide_input, narrow_input)]
    pushed = times(coef, [jnp.dot(drive_now, w, preferred_element_type=F32) for w in weights])
    push_r[...] = pushed[0]
    push_i[...] = pushed[1]
    wide_base = [jnp.broadcast_to(b, (LANES, STATES)) for b in base]

    def scan_step(step, state):
        rows = pl.ds(pl.multiple_of(step * LANES, LANES), LANES)
        fade = decay[rows]
        grown = times(wide_base, state[:2])
        new = fade * grown[0] + push_r[rows], fade * grown[1] + push_i[rows], fade * state[2]
        push_r[rows], push_i[rows], decay[rows] = new
        return new

    zero = jnp.zeros((LANES, STATES), F32)
    end_r, end_i, total = lax.fori_loop(0, STEPS, scan_step, (zero, zero, zero + 1.0), unroll=4)
    powers = [base]
    for _ in range(5):
        powers.append(times(powers[-1], powers[-1]))
    run_base = times(powers[5], powers[4])
    _, last = chain((zero[:1], zero[:1]), (end_r, end_i), total, run_base)
    fade_all = total[:1]
    for run in range(1, LANES):
        fade_all = fade_all * total[run : run + 1]
    device_base = run_base
    for _ in range(3):
        device_base = times(device_base, device_base)
    line_base = device_base
    for _ in range(3):
        line_base = times(line_base, line_base)

    for copy in local:
        copy.wait()
    pl.semaphore_wait(barrier, 21)

    message(ymsg, y, last, fade_all)
    for step in range(1, 8):
        send(ymsg.at[y], ymsg.at[y], m_send.at[1], m_recv.at[1], along_y(step))
    held_values = {}

    def start_rest():
        gather_start(mats, 0)
        gains[tp] = mix_gain[...]
        for step in range(1, 8):
            send(mix_gain, gains.at[tp], m_send.at[0], m_recv.at[0], group(step))

    def do_ywait():
        arrived(ymsg.at[pl.ds(0, 7)], m_recv.at[1])
        zrow, onerow = zero[:1], zero[:1] + 1.0
        whole, before = (zrow, zrow), (zrow, zrow)
        whole_fade, before_fade, before_base = onerow, onerow, (onerow, zrow)
        for k in range(8):
            got = ymsg[k]
            fade = got[2:3]
            grown = times(device_base, whole)
            new = fade * grown[0] + got[0:1], fade * grown[1] + got[1:2]
            new_fade = whole_fade * fade
            new_base = times(before_base, device_base)
            earlier = k < y
            before = [jnp.where(earlier, n, o) for n, o in zip(new, before)]
            before_fade = jnp.where(earlier, new_fade, before_fade)
            before_base = [jnp.where(earlier, n, o) for n, o in zip(new_base, before_base)]
            whole, whole_fade = new, new_fade

        message(zmsg, z, whole, whole_fade)
        for step in range(1, 8):
            send(zmsg.at[z], zmsg.at[z], m_send.at[2], m_recv.at[2], along_z(step))
        held_values["before"] = before, before_fade, before_base

    def do_zwait():
        arrived(zmsg.at[pl.ds(0, 7)], m_recv.at[2])
        before, before_fade, before_base = held_values["before"]
        zrow = zero[:1]
        enter = (zrow, zrow)
        for k in range(8):
            got = zmsg[k]
            grown = times(line_base, enter)
            new = got[2:3] * grown[0] + got[0:1], got[2:3] * grown[1] + got[1:2]
            enter = [jnp.where(k < z, n, o) for n, o in zip(new, enter)]
        grown = times(before_base, enter)
        enter = before_fade * grown[0] + before[0], before_fade * grown[1] + before[1]

        held_values["enter"] = enter

    def do_readout():
        enter = held_values["enter"]
        starts, _ = chain(enter, (end_r, end_i), total, run_base)

        def fix_step(step, state):
            rows = pl.ds(pl.multiple_of(step * LANES, LANES), LANES)
            state = times(wide_base, state)
            push_r[rows] = push_r[rows] + decay[rows] * state[0]
            push_i[rows] = push_i[rows] + decay[rows] * state[1]
            return state

        lax.fori_loop(0, STEPS, fix_step, tuple(starts), unroll=4)
        real_block, imag_block = blocks(wide_output, narrow_output)
        response = lax.dot_general(push_r[...].astype(BF), real_block.astype(BF), NT, preferred_element_type=F32)
        response -= lax.dot_general(push_i[...].astype(BF), imag_block.astype(BF), NT, preferred_element_type=F32)
        response += skip[...] * drive_now.astype(F32)
        active = 0.5 * response * (1.0 + lax.erf(response * (0.5**0.5)))
        active = jnp.dot(back_order(), active.astype(BF), preferred_element_type=F32).astype(BF)

        act_out[...] = active.reshape(8, 48, 128)
        act_in[tp] = act_out[tp]
        for step in range(1, 8):
            to = group(step)
            send(act_out.at[to[1]], act_in.at[tp], m_send.at[3], m_recv.at[3], to)

    def do_act():
        arrived(gains.at[pl.ds(0, 7)], m_recv.at[0])
        arrived(act_in.at[pl.ds(0, 7)], m_recv.at[3])
        rows = jnp.concatenate([act_in[k] for k in range(8)], axis=1).astype(F32)
        gain = jnp.concatenate([gains[k] for k in range(8)], axis=1)
        power = jnp.sum(rows * rows, axis=1, keepdims=True) * (1.0 / 1024)
        held_values["mixed"] = (rows * lax.rsqrt(power + EPS) * gain).astype(BF)

    def do_proj():
        gather_partner(mats, 0)
        for n in range(8):
            cols = pl.ds(n * 256, 256)
            proj = jnp.dot(held_values["mixed"], mats[:, :, cols].reshape(1024, 256), preferred_element_type=F32)
            carried[:, cols] = (own_in[:, cols].astype(F32) + proj).astype(BF)
        values = carried[...].astype(F32)
        power = jnp.sum(values * values, axis=1, keepdims=True) * (1.0 / 2048)
        normed[tp] = (values * lax.rsqrt(power + EPS) * mlp_gain[...]).astype(BF)
        gather_start(normed, 1)

    def do_up():
        gather_partner(normed, 1)
        for n in range(4):
            cols = pl.ds((n % 2) * 256, 256)
            buf = bufs[n // 2]
            if n < 2:
                weight = buf[:, :, cols].reshape(2048, 256)
            else:
                weight = jnp.concatenate([buf[(s % 8) * 8 + s // 8, :, cols] for s in range(64)], axis=0)
            pre = jnp.dot(normed[...].reshape(384, 2048), weight, preferred_element_type=F32)
            pre = jnp.maximum(pre, 0.0)
            squared[:, pl.ds(n * 256, 256)] = (pre * pre).astype(BF)

    def chip(step):
        return (x + step + 4) % 4

    def halves_of(c):
        half = len(CHUNKS[c]) * 128
        return pl.ds(0, half), pl.ds(half, half)

    def unit(c, k):
        return mod8(z + OFFSETS[CHUNKS[c][k]])

    def do_product(c):
        for k in range(len(CHUNKS[c])):
            q = unit(c, k)
            first = dn_a[pl.ds(pl.multiple_of(q * 8, 8), 8)].reshape(256, 512)
            second = jnp.concatenate([dn_b[s * 8 + q] for s in range(8)], axis=0)
            piece = lax.dot_general(squared[:, :512], first, NT, preferred_element_type=F32)
            piece += lax.dot_general(squared[:, 512:], second, NT, preferred_element_type=F32)
            piece = piece.astype(BF)
            for b in range(8):
                part[c][(b % 2) * 4 + b // 2, :, pl.ds(k * 256, 256)] = piece[b * 48 : (b + 1) * 48]
        send(part[c].at[pl.ds((1 - core) * 4, 4)], pair_in[c], t_send.at[c], t_recv.at[c, 0], partner)

    def chip_sum(c, step, cols=slice(None)):
        at = chip(step)
        return part[c][core * 4 + at, :, cols].astype(F32) + pair_in[c][at, :, cols].astype(F32)

    def do_sum(c):
        arrived(pair_in[c], t_recv.at[c, 0])
        if c in DIRECT:
            for n, step in enumerate((2, 1, -1)):
                acc[c][n] = chip_sum(c, step).astype(BF)
                send(acc[c].at[n], side_in[c].at[n], t_send.at[c], t_recv.at[c, 3], along_x(step))
            return
        cut = halves_of(c)
        acc[c][0] = chip_sum(c, 2).astype(BF)
        for n, direction in enumerate((1, -1)):
            send(acc[c].at[0, :, cut[n]], half_in[c].at[n], t_send.at[c], t_recv.at[c, 1 + n], along_x(direction))
        for n, direction in enumerate((1, -1)):
            ready = cut[1 - n]
            acc[c][1 + n, :, ready] = chip_sum(c, direction, ready).astype(BF)
            send(
                acc[c].at[1 + n, :, ready], side_in[c].at[n, :, ready],
                t_send.at[c], t_recv.at[c, 3], along_x(direction),
            )

    def do_on(c):
        cut = halves_of(c)
        for n, direction in enumerate((1, -1)):
            arrived(half_in[c].at[n], t_recv.at[c, 1 + n])
            acc[c][1 + n, :, cut[n]] = (chip_sum(c, direction, cut[n]) + half_in[c][n].astype(F32)).astype(BF)
            send(
                acc[c].at[1 + n, :, cut[n]], side_in[c].at[n, :, cut[n]],
                t_send.at[c], t_recv.at[c, 3], along_x(direction),
            )

    def do_done(c):
        cols = [carried[:, pl.ds(pl.multiple_of(unit(c, k) * 256, 256), 256)] for k in range(len(CHUNKS[c]))]
        mine = chip_sum(c, 0) + jnp.concatenate(cols, axis=1).astype(F32)
        arrived(side_in[c], t_recv.at[c, 3])
        for n in range(3 if c in DIRECT else 2):
            mine += side_in[c][n].astype(F32)
        final[c][tp] = mine.astype(BF)
        ref = final[c].at[tp]
        for n, step in enumerate((1, -1, 2) if c in DIRECT else (1, -1)):
            send(ref, ref, t_send.at[c], t_recv.at[c, 4 + n], along_x(step))
        send(ref, ref, t_send.at[c], t_recv.at[c, 8], partner)

    def do_pass(c):
        for n, step in enumerate((1, -1, 2) if c in DIRECT else (1, -1)):
            ref = final[c].at[along_x(-step)[1]]
            arrived(ref, t_recv.at[c, 4 + n])
            if c not in DIRECT:
                piece = ref.at[:, halves_of(c)[n]]
                send(piece, piece, t_send.at[c], t_recv.at[c, 6 + n], along_x(step))
            send(ref, ref, t_send.at[c], t_recv.at[c, 8], partner)

    def do_last(c):
        for n in range(2):
            piece = final[c].at[along_x(2)[1], :, halves_of(c)[n]]
            arrived(piece, t_recv.at[c, 6 + n])
            send(piece, piece, t_send.at[c], t_recv.at[c, 8], partner)

    def out_copy(c, k):
        cols = pl.ds(pl.multiple_of(unit(c, k) * 256, 256), 256)
        return pltpu.make_async_copy(
            final[c].at[:, :, pl.ds(k * 256, 256)], out.at[:, :, cols], out_sem.at[CHUNKS[c][k]]
        )

    def do_out(c):
        arrived(final[c].at[pl.ds(0, 4)], t_recv.at[c, 8])
        for k in range(len(CHUNKS[c])):
            out_copy(c, k).start()

    def do_clean():
        for n in range(4):
            left(bufs[n].at[pl.ds(0, 63)], w_send.at[n])
        left(gains.at[pl.ds(0, 7)], m_send.at[0])
        left(ymsg.at[pl.ds(0, 7)], m_send.at[1])
        left(zmsg.at[pl.ds(0, 7)], m_send.at[2])
        left(act_out.at[pl.ds(0, 7)], m_send.at[3])
        left(mats.at[pl.ds(0, 7)], ag_send.at[0])
        left(normed.at[pl.ds(0, 7)], ag_send.at[1])

    do = {
        "ywait": do_ywait, "zwait": do_zwait, "readout": do_readout, "act": do_act, "proj": do_proj, "up": do_up,
        "clean": do_clean,
        "mats0": lambda: gather_middle(mats, 0, (0,)), "mats1": lambda: gather_middle(mats, 0, (1,)),
        "mats2": lambda: gather_end(mats, 0),
        "rows0": lambda: gather_middle(normed, 1, (0,)), "rows1": lambda: gather_middle(normed, 1, (1,)),
        "rows2": lambda: gather_end(normed, 1),
    }
    by_chunk = {
        "product": do_product, "sum": do_sum, "on": do_on, "done": do_done, "pass": do_pass, "last": do_last,
        "out": do_out,
    }
    started = False
    for kind, what in plan()[0]:
        if kind == "wait" and not started:
            started = True
            start_rest()
        if kind == "send":
            copy_send(what)
        elif kind == "wait":
            copy_wait(what)
        else:
            if what in do:
                do[what]()
            else:
                by_chunk[what[:-1]](int(what[-1]))
    for c, chunk in enumerate(CHUNKS):
        for k in range(len(chunk)):
            out_copy(c, k).wait()
        left(part[c], t_send.at[c])


def step(*args):
    args = list(args)
    for n in (10, 11, 13):
        args[n] = args[n].reshape(1, -1)
    args[4] = args[4].T
    for n in (6, 7):
        args[n] = jnp.swapaxes(args[n], 2, 3)
    vmem, hbm = pl.BlockSpec(memory_space=pltpu.VMEM), pl.BlockSpec(memory_space=pltpu.HBM)
    dma = pltpu.SemaphoreType.DMA
    scratch = [
        *[pltpu.VMEM((64, 32, 512), BF)] * 4,
        pltpu.VMEM((8, 128, 2048), BF),
        pltpu.VMEM((8, 48, 2048), BF),
        pltpu.VMEM((48, 2048), BF),
        pltpu.VMEM((48, 2048), BF),
        *[pltpu.VMEM((384, STATES), F32)] * 3,
        *[pltpu.VMEM((8, 4, STATES), F32)] * 2,
        pltpu.VMEM((8, 1, 128), F32),
        pltpu.VMEM((8, 48, 128), BF),
        pltpu.VMEM((8, 48, 128), BF),
        pltpu.VMEM((384, 1024), BF),
        dma((6,)), dma((4,)), dma((4, 4)), dma((4, 32)), dma((4,)), dma((4,)),
        dma((2,)), dma((2, 7)), dma((4,)), dma((4, 9)), dma((8,)),
    ]
    for c, chunk in enumerate(CHUNKS):
        width = 256 * len(chunk)
        final = c in DIRECT
        scratch += [
            pltpu.VMEM((14, 48, width), BF),
            pltpu.VMEM((4, 48, width), BF),
            pltpu.VMEM((3, 48, width), BF),
            pltpu.VMEM((2, 48, width // 2), BF),
            pltpu.VMEM((3 if final else 2, 48, width), BF),
            pltpu.VMEM((8, 48, width), BF),
        ]
    whole = pl.pallas_call(
        kernel,
        out_shape=jax.ShapeDtypeStruct((8, 48, 2048), BF),
        in_specs=[hbm if n in (0, 12, 14, 15) else vmem for n in range(16)],
        out_specs=hbm,
        scratch_shapes=scratch,
        compiler_params=pltpu.CompilerParams(
            collective_id=0, has_side_effects=True, vmem_limit_bytes=58 * 1024 * 1024
        ),
    )(*args)
    return whole.reshape(384, 2048)


def solution(mesh):
    return jax.shard_map(
        step,
        mesh=mesh,
        in_specs=(
            P("sp", None),
            P("sp", "tp"),
            P(None, "tp", None),
            P(None, "tp", None),
            P("tp", None),
            P("tp", None, "sp"),
            P(None, "tp", None, None),
            P(None, "tp", None, None),
            P(None, "tp", None, None),
            P(None, "tp", None, None),
            P("tp"),
            P("tp"),
            P("tp", None),
            P(),
            P("sp", "tp"),
            P("sp", "tp"),
        ),
        out_specs=P("sp", None),
        check_vma=False,
    )
```

time: 102 us -> 89.8 us (0.88)
  Pallas kernels: 99.4 us -> 86.9 us
    pallas_call x1, Pallas kernels: 99.4 us -> 86.9 us  [step(): pl.pallas_call(kernel, out_shape=jax.ShapeDtypeStruct((8, 48, 2048), BF),...]
where the time goes in v3:
time: 89.8 us; the launch traced here: 89.6 us
  Pallas kernels  86.9 us (97%)
  local copies, waits for them, and re-layouts  2.73 us (3%)
    pallas_call x1, Pallas kernels, step(): pl.pallas_call(kernel, out_shape=jax.ShapeDtypeStruct((8, 48, 2048), BF),...  86.9 us
    unnamed x1, local copies, waits for them, and re-layouts  2.73 us

profile of v3, /device:TPU:1, one launch (start us, length us, event | category | flops | bytes accessed | tf_op | source)
XLA Modules:
  0.0 89.6 jit_solution(12078159121310930224)
XLA Ops:
  0.0 86.9 %shard_map.154 = bf16[8,48,2048]{2,1,0:T(8,128)(2,1)} custom-call(bf16[384,2048]{1,0:T(8,128)(2,1)} %hidden_in.1, bf16[384,128]{1,0:T(8,128)(2,1)} %drive.1, f32[2,4,64]{2,1,0:T(4,128)} %wide_poles.1, f32[2,4,32]{2,1,0:T(4,128)} %narrow_poles.1, f32[2,4]{1,0:T(2,128)} %bitcast.11, f32[4,2,384]{2,1,0:T(2,128)} %forget.1, bf16[2,4,16,64]{3,2,1,0:T(8,128)(2,1)} %bitcast.8, ...), custom_call_target="tpu_custom_call" | custom-call | tf_op jit(solution)/shard_map/pallas_call | solution.py:693
  86.9 2.7 %copy.18 = bf16[384,2048]{1,0:T(8,128)(2,1)} copy(bf16[384,2048]{1,0:T(8,128)(2,1)} %bitcast.7) | data formatting | bytes 3145728

commit v4 on v3

--- a/solution.py
+++ b/solution.py
@@ -602,16 +602,11 @@
             arrived(piece, t_recv.at[c, 6 + n])
             send(piece, piece, t_send.at[c], t_recv.at[c, 8], partner)
 
-    def out_copy(c, k):
-        cols = pl.ds(pl.multiple_of(unit(c, k) * 256, 256), 256)
-        return pltpu.make_async_copy(
-            final[c].at[:, :, pl.ds(k * 256, 256)], out.at[:, :, cols], out_sem.at[CHUNKS[c][k]]
-        )
-
     def do_out(c):
         arrived(final[c].at[pl.ds(0, 4)], t_recv.at[c, 8])
         for k in range(len(CHUNKS[c])):
-            out_copy(c, k).start()
+            cols = pl.ds(pl.multiple_of(unit(c, k) * 256, 256), 256)
+            out[:, :, cols] = final[c][:, :, pl.ds(k * 256, 256)]
 
     def do_clean():
         for n in range(4):
@@ -650,8 +645,6 @@
             else:
                 by_chunk[what[:-1]](int(what[-1]))
     for c, chunk in enumerate(CHUNKS):
-        for k in range(len(chunk)):
-            out_copy(c, k).wait()
         left(part[c], t_send.at[c])
 
 
@@ -662,6 +655,7 @@
     args[4] = args[4].T
     for n in (6, 7):
         args[n] = jnp.swapaxes(args[n], 2, 3)
+    args = [pltpu.with_memory_space_constraint(a, pltpu.HBM) for a in args]
     vmem, hbm = pl.BlockSpec(memory_space=pltpu.VMEM), pl.BlockSpec(memory_space=pltpu.HBM)
     dma = pltpu.SemaphoreType.DMA
     scratch = [
@@ -694,10 +688,10 @@
         kernel,
         out_shape=jax.ShapeDtypeStruct((8, 48, 2048), BF),
         in_specs=[hbm if n in (0, 12, 14, 15) else vmem for n in range(16)],
-        out_specs=hbm,
+        out_specs=vmem,
         scratch_shapes=scratch,
         compiler_params=pltpu.CompilerParams(
-            collective_id=0, has_side_effects=True, vmem_limit_bytes=58 * 1024 * 1024
+            collective_id=0, has_side_effects=True, vmem_limit_bytes=48 * 1024 * 1024
         ),
     )(*args)
     return whole.reshape(384, 2048)

time: 89.8 us -> 87.4 us (0.973)
  local copies, waits for them, and re-layouts: 2.73 us -> 1.15 us
  Pallas kernels: 86.9 us -> 86 us
    unnamed x1, local copies, waits for them, and re-layouts: 2.73 us -> 1.15 us
where the time goes in v4:
time: 87.4 us; the launch traced here: 87.2 us
  Pallas kernels  86 us (98%)
  local copies, waits for them, and re-layouts  1.15 us (1%)
    pallas_call x1, Pallas kernels, step(): pl.pallas_call(kernel, out_shape=jax.ShapeDtypeStruct((8, 48, 2048), BF),...  86 us

profile of v4, /device:TPU:1, one launch (start us, length us, event | category | flops | bytes accessed | tf_op | source)
XLA Modules:
  0.0 87.2 jit_solution(6533110254102833641)
XLA Ops:
  0.0 86.0 %shard_map.154 = bf16[8,48,2048]{2,1,0:T(8,128)(2,1)S(1)} custom-call(bf16[384,2048]{1,0:T(8,128)(2,1)} %hidden_in.1, bf16[384,128]{1,0:T(8,128)(2,1)} %drive.1, f32[2,4,64]{2,1,0:T(4,128)} %wide_poles.1, f32[2,4,32]{2,1,0:T(4,128)} %narrow_poles.1, f32[2,4]{1,0:T(2,128)} %bitcast.11, f32[4,2,384]{2,1,0:T(2,128)} %forget.1, bf16[2,4,16,64]{3,2,1,0:T(8,128)(2,1)} %bitcast.8, ...), custom_call_target="tpu_custom_call" | custom-call | tf_op jit(solution)/shard_map/pallas_call | solution.py:687
  86.1 1.1 %copy.18 = bf16[384,2048]{1,0:T(8,128)(2,1)} copy(bf16[384,2048]{1,0:T(8,128)(2,1)S(1)} %bitcast.7) | data formatting | bytes 3145728

commit v5 on v4

--- a/solution.py
+++ b/solution.py
@@ -115,15 +115,16 @@
 
 
 OFFSETS = (0, -1, 1, -2, 2, -3, 3, 4)
-RIGHTWARD = (0, 1, 4, 5)
+GROUPS = ((0,), (1, 2), (3, 4), (5, 6), (7,))
+RIGHTWARD = (0, 1, 3, 5)
 CHUNKS = ((0, 1, 2), (3, 4), (5, 6), (7,))
 DIRECT = (2, 3)
-COPY, DELAY, ISSUE, AHEAD = 0.703, 2.2, 0.03, 2.5
-DUE = (32.0, 36.0, 42.0, 46.0)
+COPY, DELAY, ISSUE, AHEAD, FILL, LATE = 0.703, 2.6, 0.03, 1.8, 1.8, 0.6
+DUE, UP_DUE = (32.0, 36.0, 42.0, 46.0), 15.0
 
 
 def chunk_of(s):
-    return [n for n, chunk in enumerate(CHUNKS) if s in chunk][0]
+    return [n for n, chunk in enumerate(CHUNKS) if GROUPS[s][0] in chunk][0]
 
 
 def slack(op):
@@ -132,7 +133,7 @@
     if kind == "first":
         return (0.0 if n < 2 else 8.0) + hop
     if n < 2:
-        return 15.0 - (4 - hop) * step
+        return UP_DUE - (4 - hop) * step
     if n == 3:
         return DUE[chunk_of(s)] - (4 - hop) * step
     return min(DUE[h - 1] - (h - hop) * step for h in range(hop, 5))
@@ -142,7 +143,7 @@
     ops = []
     if chunk is None or chunk == 0:
         ops += [("first", n, 0, hop) for hop in range(1, 5)]
-    for s in range(8):
+    for s in range(len(GROUPS)):
         for hop in range(1, 5):
             mine = chunk is None or (hop == chunk + 1 if n == 2 else chunk_of(s) == chunk)
             if mine:
@@ -153,12 +154,13 @@
 def steps_of():
     ups = waits_of(0) | waits_of(1)
     steps = {
-        "ywait": ((), 4.3, 0.1, set()),
-        "zwait": (("ywait",), 4.5, 0.1, set()),
+        "local": ((), 0.0, 1.8, set()),
+        "ywait": (("local",), 6.0, 0.1, set()),
+        "zwait": (("ywait",), 8.0, 0.1, set()),
         "readout": (("zwait",), 0.0, 1.3, set()),
-        "mats0": ((), 8.5, 0.05, set()),
+        "mats0": (("local",), 8.0, 0.05, set()),
         "mats1": (("mats0",), 5.6, 0.05, set()),
-        "act": (("readout", "mats1"), 3.5, 0.2, set()),
+        "act": (("readout", "mats1"), 5.5, 0.2, set()),
         "mats2": (("mats1",), 5.0, 0.05, set()),
         "proj": (("act", "mats2"), 1.3, 1.0, set()),
         "rows0": (("proj",), 4.3, 0.05, set()),
@@ -185,7 +187,7 @@
 
 def plan():
     steps, order = steps_of(), []
-    free, ready, coming = [1.0, 0.0], [set(), set()], []
+    free, ready, coming = [LATE, LATE], [set(), set()], []
     ended, seen, now = {}, set(), 0.0
 
     def link(op):
@@ -199,16 +201,19 @@
         offer(("line", n, 0, 1))
     while steps or coming or ready[0] or ready[1]:
         for side in range(2):
-            ahead = AHEAD
+            ahead = 0.0
             for name, (before, after, own, needs) in steps.items():
                 if own > 0.9 and all(b in ended for b in before) and needs <= seen:
                     if max([ended[b] for b in before], default=0.0) + after < now + 0.3:
-                        ahead = AHEAD + own
-            while ready[side] and free[side] - now < ahead:
+                        ahead = own
+            while ready[side]:
                 op = min(ready[side], key=lambda o: (slack(o), o))
+                if free[side] - now >= (1.0 + LATE if "local" not in ended else ahead + (AHEAD if op[1] < 2 else FILL)):
+                    break
                 ready[side].remove(op)
                 order.append(("send", op))
                 both = 1.0 if op[3] < 4 else 0.5
+                both *= 1 if op[0] == "first" else len(GROUPS[op[2]])
                 free[side] = max(free[side], now) + COPY * both
                 coming.append((free[side] + DELAY, op))
                 now += ISSUE
@@ -229,32 +234,33 @@
             if hop < 4:
                 offer((kind, n, s, hop + 1))
             if kind == "first":
-                for k, offset in enumerate(OFFSETS):
-                    if abs(offset) == hop:
-                        offer(("line", n, k, 1))
+                offer(("line", n, hop, 1))
         elif step:
-            wake = [free[side] - AHEAD * 0.5 for side in range(2) if ready[side]]
+            wake = [free[side] - FILL * 0.5 for side in range(2) if ready[side]]
             if wake and min(wake) < step[0] and min(wake) > now:
                 now = min(wake)
                 continue
             now = max(now, step[0]) + steps[step[1]][2]
             ended[step[1]] = now
             order.append(("step", step[1]))
-            if step[1] == "ywait":
-                free[1] = max(free[1], now) + 1.0
+            if step[1] in ("local", "ywait"):
+                side = int(step[1] == "ywait")
+                free[side] = max(free[side], now) + 1.0
             del steps[step[1]]
         else:
-            now = max(now, min(free[side] for side in range(2) if ready[side]) - AHEAD * 0.5)
+            now = max(now, min(free[side] for side in range(2) if ready[side]) - FILL * 0.5)
     return order, ended, now
 
 
 def kernel(
-    hidden_in, drive, wide_poles, narrow_poles, log_step, forget, wide_input, narrow_input,
-    wide_output, narrow_output, skip, mix_gain, out_weight, mlp_gain, up_weight, down_weight,
+    hidden_in, drive_in, wide_poles_in, narrow_poles_in, log_step_in, forget_in, wide_input_in, narrow_input_in,
+    wide_output_in, narrow_output_in, skip_in, mix_gain_in, out_weight, mlp_gain_in, up_weight, down_weight,
     out,
+    drive, wide_poles, narrow_poles, log_step, forget, wide_input, narrow_input,
+    wide_output, narrow_output, skip, mix_gain, mlp_gain,
     up_a, up_b, dn_a, dn_b, mats, normed, own_in, carried,
     push_r, push_i, decay, ymsg, zmsg, gains, act_out, act_in, squared,
-    loc_sem, w_send, s1_recv, s2_recv, m_send, m_recv, ag_send, ag_recv, t_send, t_recv, out_sem,
+    loc_sem, w_send, s1_recv, s2_recv, m_send, m_recv, ag_send, ag_recv, t_send, t_recv,
     *pieces,
 ):
     part, pair_in, acc, half_in, side_in, final = (pieces[n :: 6] for n in range(6))
@@ -314,7 +320,14 @@
         )
     local.append(pltpu.make_async_copy(out_weight, mats.at[tp], loc_sem.at[4]))
     local.append(pltpu.make_async_copy(hidden_in.at[pl.ds(pl.multiple_of(tp * 48, 16), 48)], own_in, loc_sem.at[5]))
-    for copy in local:
+    small = (
+        (drive_in, drive), (wide_poles_in, wide_poles), (narrow_poles_in, narrow_poles), (log_step_in, log_step),
+        (forget_in, forget), (wide_input_in, wide_input), (narrow_input_in, narrow_input),
+        (wide_output_in, wide_output), (narrow_output_in, narrow_output), (skip_in, skip),
+        (mix_gain_in, mix_gain), (mlp_gain_in, mlp_gain),
+    )
+    fetched = [pltpu.make_async_copy(src, dst, loc_sem.at[6 + n]) for n, (src, dst) in enumerate(small)]
+    for copy in local[:4] + fetched + local[4:]:
         copy.start()
     def first_send(n, hop):
         at, line, go, _ = where_of(n)
@@ -324,10 +337,11 @@
 
     def line_send(n, s, hop):
         at, line, _, go = where_of(n)
-        for direction in (1, -1):
-            if hop < 4 or (s in RIGHTWARD) == (direction > 0):
-                ref = shard(n, mod8(at + OFFSETS[s]), mod8(line - direction * (hop - 1)))
-                send(ref, ref, w_send.at[n], s2_recv.at[n, 4 * s + hop - 1], go(direction))
+        for k in GROUPS[s]:
+            for direction in (1, -1):
+                if hop < 4 or (k in RIGHTWARD) == (direction > 0):
+                    ref = shard(n, mod8(at + OFFSETS[k]), mod8(line - direction * (hop - 1)))
+                    send(ref, ref, w_send.at[n], s2_recv.at[n, 4 * s + hop - 1], go(direction))
 
     def copy_send(op):
         kind, n, s, hop = op
@@ -339,7 +353,8 @@
     def copy_wait(op):
         kind, n, s, hop = op
         sem = s1_recv.at[n, hop - 1] if kind == "first" else s2_recv.at[n, 4 * s + hop - 1]
-        arrived(bufs[n].at[pl.ds(0, 2 if hop < 4 else 1)], sem)
+        count = (2 if hop < 4 else 1) * (1 if kind == "first" else len(GROUPS[s]))
+        arrived(bufs[n].at[pl.ds(0, count)], sem)
 
     halves = (pl.ds(0, 1024), pl.ds(1024, 1024))
 
@@ -375,58 +390,62 @@
     def message(buf, at, state, fade):
         buf[at] = jnp.concatenate([state[0], state[1], fade, fade], axis=0)
 
-    pick = order()
-    decay[...] = decay_rows(forget, pick)
-    drive_now = jnp.dot(pick, drive[...], preferred_element_type=F32).astype(BF)
-    base, coef = discretize(wide_poles, narrow_poles, log_step)
-    weights = [b.astype(BF) for b in blocks(wide_input, narrow_input)]
-    pushed = times(coef, [jnp.dot(drive_now, w, preferred_element_type=F32) for w in weights])
-    push_r[...] = pushed[0]
-    push_i[...] = pushed[1]
-    wide_base = [jnp.broadcast_to(b, (LANES, STATES)) for b in base]
-
-    def scan_step(step, state):
-        rows = pl.ds(pl.multiple_of(step * LANES, LANES), LANES)
-        fade = decay[rows]
-        grown = times(wide_base, state[:2])
-        new = fade * grown[0] + push_r[rows], fade * grown[1] + push_i[rows], fade * state[2]
-        push_r[rows], push_i[rows], decay[rows] = new
-        return new
-
-    zero = jnp.zeros((LANES, STATES), F32)
-    end_r, end_i, total = lax.fori_loop(0, STEPS, scan_step, (zero, zero, zero + 1.0), unroll=4)
-    powers = [base]
-    for _ in range(5):
-        powers.append(times(powers[-1], powers[-1]))
-    run_base = times(powers[5], powers[4])
-    _, last = chain((zero[:1], zero[:1]), (end_r, end_i), total, run_base)
-    fade_all = total[:1]
-    for run in range(1, LANES):
-        fade_all = fade_all * total[run : run + 1]
-    device_base = run_base
-    for _ in range(3):
-        device_base = times(device_base, device_base)
-    line_base = device_base
-    for _ in range(3):
-        line_base = times(line_base, line_base)
-
-    for copy in local:
+    for copy in local[:4]:
         copy.wait()
     pl.semaphore_wait(barrier, 21)
-
-    message(ymsg, y, last, fade_all)
-    for step in range(1, 8):
-        send(ymsg.at[y], ymsg.at[y], m_send.at[1], m_recv.at[1], along_y(step))
     held_values = {}
 
-    def start_rest():
+    def do_local():
+        for copy in fetched + local[4:]:
+            copy.wait()
+        pick = order()
+        decay[...] = decay_rows(forget, pick)
+        drive_now = jnp.dot(pick, drive[...], preferred_element_type=F32).astype(BF)
+        base, coef = discretize(wide_poles, narrow_poles, log_step)
+        weights = [b.astype(BF) for b in blocks(wide_input, narrow_input)]
+        pushed = times(coef, [jnp.dot(drive_now, w, preferred_element_type=F32) for w in weights])
+        push_r[...] = pushed[0]
+        push_i[...] = pushed[1]
+        wide_base = [jnp.broadcast_to(b, (LANES, STATES)) for b in base]
+
+        def scan_step(step, state):
+            rows = pl.ds(pl.multiple_of(step * LANES, LANES), LANES)
+            fade = decay[rows]
+            grown = times(wide_base, state[:2])
+            new = fade * grown[0] + push_r[rows], fade * grown[1] + push_i[rows], fade * state[2]
+            push_r[rows], push_i[rows], decay[rows] = new
+            return new
+
+        zero = jnp.zeros((LANES, STATES), F32)
+        end_r, end_i, total = lax.fori_loop(0, STEPS, scan_step, (zero, zero, zero + 1.0), unroll=4)
+        powers = [base]
+        for _ in range(5):
+            powers.append(times(powers[-1], powers[-1]))
+        run_base = times(powers[5], powers[4])
+        _, last = chain((zero[:1], zero[:1]), (end_r, end_i), total, run_base)
+        fade_all = total[:1]
+        for run in range(1, LANES):
+            fade_all = fade_all * total[run : run + 1]
+        device_base = run_base
+        for _ in range(3):
+            device_base = times(device_base, device_base)
+        line_base = device_base
+        for _ in range(3):
+            line_base = times(line_base, line_base)
+
+
+        message(ymsg, y, last, fade_all)
+        for step in range(1, 8):
+            send(ymsg.at[y], ymsg.at[y], m_send.at[1], m_recv.at[1], along_y(step))
         gather_start(mats, 0)
         gains[tp] = mix_gain[...]
         for step in range(1, 8):
             send(mix_gain, gains.at[tp], m_send.at[0], m_recv.at[0], group(step))
+        held_values["local"] = zero, wide_base, end_r, end_i, total, run_base, device_base, line_base, drive_now
 
     def do_ywait():
         arrived(ymsg.at[pl.ds(0, 7)], m_recv.at[1])
+        zero, _, _, _, _, _, device_base, _, _ = held_values["local"]
         zrow, onerow = zero[:1], zero[:1] + 1.0
         whole, before = (zrow, zrow), (zrow, zrow)
         whole_fade, before_fade, before_base = onerow, onerow, (onerow, zrow)
@@ -451,6 +470,7 @@
     def do_zwait():
         arrived(zmsg.at[pl.ds(0, 7)], m_recv.at[2])
         before, before_fade, before_base = held_values["before"]
+        zero, _, _, _, _, _, _, line_base, _ = held_values["local"]
         zrow = zero[:1]
         enter = (zrow, zrow)
         for k in range(8):
@@ -465,6 +485,7 @@
 
     def do_readout():
         enter = held_values["enter"]
+        _, wide_base, end_r, end_i, total, run_base, _, _, drive_now = held_values["local"]
         starts, _ = chain(enter, (end_r, end_i), total, run_base)
 
         def fix_step(step, state):
@@ -619,7 +640,7 @@
         left(normed.at[pl.ds(0, 7)], ag_send.at[1])
 
     do = {
-        "ywait": do_ywait, "zwait": do_zwait, "readout": do_readout, "act": do_act, "proj": do_proj, "up": do_up,
+        "local": do_local, "ywait": do_ywait, "zwait": do_zwait, "readout": do_readout, "act": do_act, "proj": do_proj, "up": do_up,
         "clean": do_clean,
         "mats0": lambda: gather_middle(mats, 0, (0,)), "mats1": lambda: gather_middle(mats, 0, (1,)),
         "mats2": lambda: gather_end(mats, 0),
@@ -630,11 +651,7 @@
         "product": do_product, "sum": do_sum, "on": do_on, "done": do_done, "pass": do_pass, "last": do_last,
         "out": do_out,
     }
-    started = False
     for kind, what in plan()[0]:
-        if kind == "wait" and not started:
-            started = True
-            start_rest()
         if kind == "send":
             copy_send(what)
         elif kind == "wait":
@@ -644,7 +661,7 @@
                 do[what]()
             else:
                 by_chunk[what[:-1]](int(what[-1]))
-    for c, chunk in enumerate(CHUNKS):
+    for c in range(len(CHUNKS)):
         left(part[c], t_send.at[c])
 
 
@@ -659,6 +676,7 @@
     vmem, hbm = pl.BlockSpec(memory_space=pltpu.VMEM), pl.BlockSpec(memory_space=pltpu.HBM)
     dma = pltpu.SemaphoreType.DMA
     scratch = [
+        *[pltpu.VMEM(a.shape, a.dtype) for n, a in enumerate(args) if n not in (0, 12, 14, 15)],
         *[pltpu.VMEM((64, 32, 512), BF)] * 4,
         pltpu.VMEM((8, 128, 2048), BF),
         pltpu.VMEM((8, 48, 2048), BF),
@@ -670,8 +688,8 @@
         pltpu.VMEM((8, 48, 128), BF),
         pltpu.VMEM((8, 48, 128), BF),
         pltpu.VMEM((384, 1024), BF),
-        dma((6,)), dma((4,)), dma((4, 4)), dma((4, 32)), dma((4,)), dma((4,)),
-        dma((2,)), dma((2, 7)), dma((4,)), dma((4, 9)), dma((8,)),
+        dma((18,)), dma((4,)), dma((4, 4)), dma((4, 20)), dma((4,)), dma((4,)),
+        dma((2,)), dma((2, 7)), dma((4,)), dma((4, 9)),
     ]
     for c, chunk in enumerate(CHUNKS):
         width = 256 * len(chunk)
@@ -687,7 +705,7 @@
     whole = pl.pallas_call(
         kernel,
         out_shape=jax.ShapeDtypeStruct((8, 48, 2048), BF),
-        in_specs=[hbm if n in (0, 12, 14, 15) else vmem for n in range(16)],
+        in_specs=[hbm] * 16,
         out_specs=vmem,
         scratch_shapes=scratch,
         compiler_params=pltpu.CompilerParams(

time: 87.4 us -> 86.1 us (0.985)
  Pallas kernels: 86 us -> 84.8 us
    pallas_call x1, Pallas kernels: 86 us -> 84.8 us  [step(): pl.pallas_call(kernel, out_shape=jax.ShapeDtypeStruct((8, 48, 2048), BF),...]
where the time goes in v5:
time: 86.1 us; the launch traced here: 86 us
  Pallas kernels  84.8 us (98%)
  local copies, waits for them, and re-layouts  1.15 us (1%)
    pallas_call x1, Pallas kernels, step(): pl.pallas_call(kernel, out_shape=jax.ShapeDtypeStruct((8, 48, 2048), BF),...  84.8 us

profile of v5, /device:TPU:1, one launch (start us, length us, event | category | flops | bytes accessed | tf_op | source)
XLA Modules:
  0.0 86.0 jit_solution(7249470050153154539)
XLA Ops:
  0.0 84.8 %shard_map.154 = bf16[8,48,2048]{2,1,0:T(8,128)(2,1)S(1)} custom-call(bf16[384,2048]{1,0:T(8,128)(2,1)} %hidden_in.1, bf16[384,128]{1,0:T(8,128)(2,1)} %drive_in.1, f32[2,4,64]{2,1,0:T(4,128)} %wide_poles_in.1, f32[2,4,32]{2,1,0:T(4,128)} %narrow_poles_in.1, f32[2,4]{1,0:T(2,128)} %bitcast.11, f32[4,2,384]{2,1,0:T(2,128)} %forget_in.1, ...), custom_call_target="tpu_custom_call" | custom-call | tf_op jit(solution)/shard_map/pallas_call | solution.py:705
  84.8 1.1 %copy.18 = bf16[384,2048]{1,0:T(8,128)(2,1)} copy(bf16[384,2048]{1,0:T(8,128)(2,1)S(1)} %bitcast.7) | data formatting | bytes 3145728

commit v6 on v5

--- a/solution.py
+++ b/solution.py
@@ -118,7 +118,7 @@
 GROUPS = ((0,), (1, 2), (3, 4), (5, 6), (7,))
 RIGHTWARD = (0, 1, 3, 5)
 CHUNKS = ((0, 1, 2), (3, 4), (5, 6), (7,))
-DIRECT = (2, 3)
+DIRECT = (0, 1, 2, 3)
 COPY, DELAY, ISSUE, AHEAD, FILL, LATE = 0.703, 2.6, 0.03, 1.8, 1.8, 0.6
 DUE, UP_DUE = (32.0, 36.0, 42.0, 46.0), 15.0
 

time: 86.1 us -> 85.4 us (level)
  no operation moved by 1% of the time
where the time goes in v6:
time: 85.4 us; the launch traced here: 85.3 us
  Pallas kernels  84.1 us (98%)
  local copies, waits for them, and re-layouts  1.15 us (1%)
    pallas_call x1, Pallas kernels, step(): pl.pallas_call(kernel, out_shape=jax.ShapeDtypeStruct((8, 48, 2048), BF),...  84.1 us

profile of v6, /device:TPU:1, one launch (start us, length us, event | category | flops | bytes accessed | tf_op | source)
XLA Modules:
  0.0 85.3 jit_solution(2144899879043949720)
XLA Ops:
  0.0 84.1 %shard_map.154 = bf16[8,48,2048]{2,1,0:T(8,128)(2,1)S(1)} custom-call(bf16[384,2048]{1,0:T(8,128)(2,1)} %hidden_in.1, bf16[384,128]{1,0:T(8,128)(2,1)} %drive_in.1, f32[2,4,64]{2,1,0:T(4,128)} %wide_poles_in.1, f32[2,4,32]{2,1,0:T(4,128)} %narrow_poles_in.1, f32[2,4]{1,0:T(2,128)} %bitcast.11, f32[4,2,384]{2,1,0:T(2,128)} %forget_in.1, ...), custom_call_target="tpu_custom_call" | custom-call | tf_op jit(solution)/shard_map/pallas_call | solution.py:705
  84.1 1.1 %copy.18 = bf16[384,2048]{1,0:T(8,128)(2,1)} copy(bf16[384,2048]{1,0:T(8,128)(2,1)S(1)} %bitcast.7) | data formatting | bytes 3145728
